TPU v7x, 256 devices: a whole 4x4x8 slice. The times are simulated.
256 devices in a mesh: sp: 32 (over z, y), tp: 4 (over x), dp: 2 (over core).
Axes of the slice: x: 4, y: 4, z: 8, core: 2. Of those that a mesh axis runs over, the one named last changes fastest.
Arguments:
- latent: bfloat16 [2, 32768, 2048], P('dp', 'sp'), may hold values from -4 to 4
- context: bfloat16 [2, 768, 2048], P('dp', 'sp'), may hold values from -6 to 6
- cond: float32 [2, 2048], P('dp'), may hold values from -6 to 6
- ctx_cond: float32 [2048], replicated, may hold values from -6 to 6
- norm_gain: float32 [2048], replicated, may hold values from 0.1 to 1.9
- mod_shift: bfloat16 [2048, 2048], P('sp', 'tp'), may hold values from -0.125 to 0.125
- mod_scale: bfloat16 [2048, 2048], P('sp', 'tp'), may hold values from -0.125 to 0.125
- mod_gate: bfloat16 [2048, 2048], P('sp', 'tp'), may hold values from -0.125 to 0.125
- w_query: bfloat16 [2048, 2048], P(None, 'tp'), may hold values from -0.125 to 0.125
- w_key: bfloat16 [2048, 512], P(None, 'tp'), may hold values from -0.125 to 0.125
- w_value: bfloat16 [2048, 512], P(None, 'tp'), may hold values from -0.125 to 0.125
- w_out: bfloat16 [2048, 2048], P('tp'), may hold values from -2 to 2
- q_gain: float32 [128], replicated, may hold values from 0.1 to 1.9
- k_gain: float32 [128], replicated, may hold values from 0.1 to 1.9
- sinks: float32 [16], P('tp'), may hold values from 3 to 8
Outputs:
- result: bfloat16 [2, 32768, 2048], P('dp', ('sp', 'tp'))
All inputs are finite; a program needn't handle non-finite values.
Results may differ from a plain program's by a relative error of at most 0.013.
Values may be sent and summed in bfloat16 or wider, within the bound.
A program may use at most 128 MiB of HBM per device.

v0:
```python
import jax
import jax.numpy as jnp
from jax import lax
from jax.sharding import PartitionSpec as P

HEAD_DIM = 128
WINDOW = 128
GRID_W = 64


NORM_EPSILON = 1e-06
ROPE_BASE = 10000.0


def from_everyone(array, axis):
    peers = lax.axis_size(axis)
    return lax.all_to_all(
        jnp.broadcast_to(array[None], (peers, *array.shape)), axis, 0, 0, tiled=True
    )


def taken_together(array, axis):
    return from_everyone(array, axis).sum(axis=0)


def in_order(pieces, dim):
    lengths = list(pieces.shape[1:])
    lengths[dim] *= pieces.shape[0]
    return jnp.moveaxis(pieces, 0, dim).reshape(lengths)


def gather_directly(array, axis, dim):
    pieces = from_everyone(array, axis)
    return in_order(pieces, dim)


def extended(array, sides, width):
    for axis, dim in sides:
        peers, length = (lax.axis_size(axis), array.shape[dim])
        up = [(i, (i + 1) % peers) for i in range(peers - 1)]
        down = [(j, i) for i, j in up]
        last = lax.slice_in_dim(array, length - width, length, axis=dim)
        first = lax.slice_in_dim(array, 0, width, axis=dim)
        before = lax.ppermute(last, axis, up)
        after = lax.ppermute(first, axis, down)
        array = jnp.concatenate([before, array, after], axis=dim)
    return array


def split_up(array, dim, peers):
    before, after = (array.shape[:dim], array.shape[dim + 1 :])
    return jnp.moveaxis(array.reshape(*before, peers, -1, *after), dim, 0)


def summed_on_arrival(array, axis, dim):
    peers = lax.axis_size(axis)
    pieces = lax.all_to_all(split_up(array, dim, peers), axis, 0, 0, tiled=True)
    return jnp.sum(pieces.astype(jnp.float32), axis=0)


def head_norm(vectors, gain_row):
    return (
        vectors
        * lax.rsqrt(jnp.mean(vectors * vectors, axis=-1, keepdims=True) + NORM_EPSILON)
        * gain_row
    )


def modulated(rows_in, gain_row, shift_row, scale_row):
    values = rows_in.astype(jnp.float32)
    normed = (
        values
        * lax.rsqrt(jnp.mean(values * values, axis=-1, keepdims=True) + NORM_EPSILON)
        * gain_row
    )
    return (normed * (1.0 + scale_row) + shift_row).astype(jnp.bfloat16)


def rotate_half(halves, coords):
    quarter = halves.shape[-1] // 2
    frequency = ROPE_BASE ** (-jnp.arange(quarter, dtype=jnp.float32) / quarter)
    angles = coords.astype(jnp.float32)[:, None] * frequency
    cosine_part = jnp.cos(angles)[:, None, :]
    sine_part = jnp.sin(angles)[:, None, :]
    first_part = halves[..., :quarter]
    second_part = halves[..., quarter:]
    return jnp.concatenate(
        [
            first_part * cosine_part - second_part * sine_part,
            second_part * cosine_part + first_part * sine_part,
        ],
        axis=-1,
    )


def rotate(vectors, positions):
    half_dim = vectors.shape[-1] // 2
    return jnp.concatenate(
        [
            rotate_half(vectors[..., :half_dim], positions // GRID_W),
            rotate_half(vectors[..., half_dim:], positions % GRID_W),
        ],
        axis=-1,
    )


def per_device(
    latent,
    context,
    cond,
    ctx_cond,
    norm_gain,
    mod_shift,
    mod_scale,
    mod_gate,
    w_query,
    w_key,
    w_value,
    w_out,
    q_gain,
    k_gain,
    sinks,
):
    tok_count = latent.shape[1]
    part_rows = mod_shift.shape[0]
    sp_index = lax.axis_index("sp")
    tp_index = lax.axis_index("tp")
    cond_rows = jnp.stack([cond[0], ctx_cond])
    own_cond = lax.dynamic_slice_in_dim(cond_rows, sp_index * part_rows, part_rows, 1)
    active = jax.nn.silu(own_cond).astype(jnp.bfloat16)
    shifts = jnp.dot(active, mod_shift, preferred_element_type=jnp.float32)
    scales = jnp.dot(active, mod_scale, preferred_element_type=jnp.float32)
    gate_rows = jnp.dot(active[0:1], mod_gate, preferred_element_type=jnp.float32)
    partial_value = jnp.concatenate([shifts, scales, gate_rows], axis=0)
    summed = taken_together(partial_value, "sp")
    modulation = gather_directly(summed, "tp", 1)
    lat_in = modulated(latent[0], norm_gain, modulation[0], modulation[2])
    ctx_in = modulated(context[0], norm_gain, modulation[1], modulation[3])
    gate_row = modulation[4]
    kv_local = w_key.shape[1] // HEAD_DIM
    q_local = w_query.shape[1] // HEAD_DIM
    group_size = q_local // kv_local
    kv_width = kv_local * HEAD_DIM
    score_scale = HEAD_DIM ** (-0.5)
    positions = sp_index * tok_count + jnp.arange(tok_count, dtype=jnp.int32)
    lat_queries = rotate(
        head_norm(
            jnp.dot(lat_in, w_query, preferred_element_type=jnp.float32).reshape(
                tok_count, q_local, HEAD_DIM
            ),
            q_gain,
        ),
        positions,
    ).astype(jnp.bfloat16)
    lat_keys = rotate(
        head_norm(
            jnp.dot(lat_in, w_key, preferred_element_type=jnp.float32).reshape(
                tok_count, kv_local, HEAD_DIM
            ),
            k_gain,
        ),
        positions,
    ).astype(jnp.bfloat16)
    lat_values = jnp.dot(lat_in, w_value, preferred_element_type=jnp.float32).astype(jnp.bfloat16)
    lat_both = jnp.concatenate([lat_keys.reshape(tok_count, kv_width), lat_values], axis=1)
    padded = extended(lat_both, (("sp", 0),), WINDOW)
    piece_keys = head_norm(
        jnp.dot(ctx_in, w_key, preferred_element_type=jnp.float32).reshape(
            ctx_in.shape[0], kv_local, HEAD_DIM
        ),
        k_gain,
    ).astype(jnp.bfloat16)
    piece_values = jnp.dot(ctx_in, w_value, preferred_element_type=jnp.float32).astype(jnp.bfloat16)
    context_both = gather_directly(
        jnp.concatenate([piece_keys.reshape(ctx_in.shape[0], kv_width), piece_values], axis=1),
        "sp",
        0,
    )
    ctx_count = context_both.shape[0]
    ctx_keys = context_both[:, :kv_width].reshape(ctx_count, kv_local, HEAD_DIM)
    ctx_values = context_both[:, kv_width:].reshape(ctx_count, kv_local, HEAD_DIM)
    block_count = tok_count // WINDOW
    padded_blocks = padded.reshape(block_count + 2, WINDOW, 2 * kv_width)
    window_both = jnp.concatenate(
        [
            padded_blocks[0:block_count],
            padded_blocks[1 : block_count + 1],
            padded_blocks[2 : block_count + 2],
        ],
        axis=1,
    )
    window_keys = window_both[..., :kv_width].reshape(block_count, 3 * WINDOW, kv_local, HEAD_DIM)
    window_values = window_both[..., kv_width:].reshape(block_count, 3 * WINDOW, kv_local, HEAD_DIM)
    query_blocks = lat_queries.reshape(block_count, WINDOW, kv_local, group_size, HEAD_DIM)
    key_rows = jnp.arange(3 * WINDOW, dtype=jnp.int32)
    query_rows = jnp.arange(WINDOW, dtype=jnp.int32)
    offset_rows = key_rows[None, :] - query_rows[:, None]
    in_band = (offset_rows >= 0) & (offset_rows <= 2 * WINDOW)
    key_pos = (
        sp_index * tok_count
        - WINDOW
        + jnp.arange(block_count, dtype=jnp.int32)[:, None] * WINDOW
        + key_rows[None, :]
    )
    seq_total = tok_count * lax.axis_size("sp")
    in_range = (key_pos >= 0) & (key_pos < seq_total)
    in_window = in_band[None, :, :] & in_range[:, None, :]
    scores = (
        jnp.einsum(
            "nqhgd,nkhd->hgnqk", query_blocks, window_keys, preferred_element_type=jnp.float32
        )
        * score_scale
    )
    weights = jnp.where(in_window[None, None], jnp.exp(scores), 0.0)
    flat_queries = lat_queries.reshape(tok_count, kv_local, group_size, HEAD_DIM)
    ctx_weights = jnp.exp(
        jnp.einsum("thgd,chd->hgtc", flat_queries, ctx_keys, preferred_element_type=jnp.float32)
        * score_scale
    )
    sink_exp = jnp.exp(sinks).reshape(kv_local, group_size)
    denominator = (
        jnp.sum(weights, axis=-1).reshape(kv_local, group_size, tok_count)
        + jnp.sum(ctx_weights, axis=-1)
        + sink_exp[:, :, None]
    )
    local_probs = (
        weights / denominator.reshape(kv_local, group_size, block_count, WINDOW)[..., None]
    ).astype(jnp.bfloat16)
    ctx_probs = (ctx_weights / denominator[..., None]).astype(jnp.bfloat16)
    local_part = jnp.einsum(
        "hgnqk,nkhd->nqhgd", local_probs, window_values, preferred_element_type=jnp.float32
    )
    ctx_part = jnp.einsum(
        "hgtc,chd->thgd", ctx_probs, ctx_values, preferred_element_type=jnp.float32
    )
    attended = (local_part.reshape(tok_count, kv_local, group_size, HEAD_DIM) + ctx_part).astype(
        jnp.bfloat16
    )
    attended = attended.reshape(tok_count, q_local * HEAD_DIM)
    sub_rows = tok_count // lax.axis_size("tp")
    mixed_rows = summed_on_arrival(
        jnp.dot(attended, w_out, preferred_element_type=jnp.float32).astype(jnp.bfloat16), "tp", 0
    )
    own_rows = lax.dynamic_slice_in_dim(latent[0], tp_index * sub_rows, sub_rows, 0).astype(
        jnp.float32
    )
    result = (own_rows + gate_row * mixed_rows).astype(jnp.bfloat16)
    return result[None]


def solution(mesh):
    in_specs = (
        P("dp", "sp", None),
        P("dp", "sp", None),
        P("dp", None),
        P(),
        P(),
        P("sp", "tp"),
        P("sp", "tp"),
        P("sp", "tp"),
        P(None, "tp"),
        P(None, "tp"),
        P(None, "tp"),
        P("tp", None),
        P(),
        P(),
        P("tp"),
    )
    out_specs = P("dp", ("sp", "tp"), None)
    return jax.shard_map(
        per_device, mesh=mesh, in_specs=in_specs, out_specs=out_specs, check_vma=False
    )
```

profile of v0, /device:TPU:32, one launch (start us, length us, event | category | flops | bytes accessed | tf_op | source)
XLA Modules:
  0.0 184.0 jit_solution(10324458758093356720)
XLA Ops:
  0.0 0.9 fusion.92
  0.9 1.0 fusion.93
  1.9 1.0 fusion.107
  2.9 1.0 fusion.106
  3.8 0.9 broadcast_in_dim.14
  4.7 11.4 %all-to-all-start = ((f32[32,5,512]{2,1,0:T(8,128)}), f32[32,5,512]{2,1,0:T(8,128)S(1)}, u32[]{:S(2)}, u32[]{:S(2)}) async-start(f32[32,5,512]{2,1,0:T(8,128)} %broadcast_in_dim.14), calls=%async_computation | async-start | bytes 1048576 | tf_op jit(solution)/shard_map/all_to_all | solution.py:17
  16.2 3.1 %fusion.3 = f32[1024]{0:T(1024)S(1)} fusion(bf16[1,1024,2048]{2,1,0:T(8,128)(2,1)} %param.15), kind=kLoop, calls=%fused_computation.8 | loop fusion | flops 6290432 | bytes 4198400 | tf_op jit(solution)/shard_map/reduce_sum | solution.py:73
  19.5 1.3 broadcast_and_fusion
  20.8 1.7 multiply_cosine_fusion.1
  22.5 10.8 %all-to-all-done = f32[32,5,512]{2,1,0:T(8,128)S(1)} async-done(((f32[32,5,512]{2,1,0:T(8,128)}), f32[32,5,512]{2,1,0:T(8,128)S(1)}, u32[]{:S(2)}, u32[]{:S(2)}) %all-to-all-start) | async-done | bytes 327712 | tf_op jit(solution)/shard_map/all_to_all | solution.py:17
  33.3 0.6 broadcast_in_dim.15
  34.0 4.3 %all-to-all-start.1 = ((f32[4,5,512]{2,1,0:T(8,128)}), f32[4,5,512]{2,1,0:T(8,128)S(1)}, u32[]{:S(2)}, u32[]{:S(2)}) async-start(f32[4,5,512]{2,1,0:T(8,128)} %broadcast_in_dim.15), calls=%async_computation.1 | async-start | bytes 131072 | tf_op jit(solution)/shard_map/all_to_all | solution.py:17
  38.3 4.0 %copy.80 = bf16[512,2048]{1,0:T(8,128)(2,1)} copy(bf16[512,2048]{0,1:T(8,128)(2,1)} %bitcast.186) | data formatting | bytes 4194304 | tf_op jit(solution)/shard_map/dot_general | solution.py:148
  42.2 1.6 all-to-all-done.1
  44.7 0.8 broadcast_in_dim.18
  45.5 5.2 %all-to-all-start.2 = ((bf16[32,24,256]{2,1,0:T(8,128)(2,1)}), bf16[32,24,256]{2,1,0:T(8,128)(2,1)}, u32[]{:S(2)}, u32[]{:S(2)}) async-start(bf16[32,24,256]{2,1,0:T(8,128)(2,1)} %broadcast_in_dim.18), calls=%async_computation.2 | async-start | bytes 786432 | tf_op jit(solution)/shard_map/all_to_all | solution.py:17
  50.7 4.2 %multiply_reduce_fusion.1 = (f32[1024]{0:T(1024)S(1)}, f32[1024,128]{0,1:T(8,128)S(1)}) fusion(bf16[2048,128]{1,0:T(8,128)(2,1)S(1)} %copy-done.10, bf16[1,1024,2048]{2,1,0:T(8,128)(2,1)} %param.15, f32[2048]{0:T(1024)S(1)} %bitcast.201, f32[2048]{0:T(1024)S(1)} %bitcast.204, f32[2048]{0:T(1024)S(1)} %copy-done.14, f32[1024]{0:T(1024)S(1)} %add_rsqrt_fusion.2), kind=kOutput, calls=%fused_computation.72 | convolution fusion | flops 549714944 | bytes 5275648 | tf_op jit(solution)/shard_map/dot_general | solution.py:157
  57.3 1.9 %fusion.35 = bf16[1024,256]{0,1:T(8,128)(2,1)S(1)} fusion(bf16[1024,256]{0,1:T(8,128)(2,1)S(1)} %bitcast_dynamic-update-slice_fusion, bf16[2048,128]{1,0:T(8,128)(2,1)S(1)} %copy-done.12, bf16[1,1024,2048]{2,1,0:T(8,128)(2,1)S(1)} %copy-done.1, f32[2048]{0:T(1024)S(1)} %bitcast.202, f32[2048]{0:T(1024)S(1)} %bitcast.205, f32[2048]{0:T(1024)S(1)} %copy-done.14, ...), kind=kOutput, calls=%fused_computation.44 | convolution fusion | flops 549584896 | bytes 5009408 | tf_op jit(solution)/shard_map/dot_general | solution.py:164
  59.2 0.7 fusion.104
  59.8 3.4 %collective-permute-start = (bf16[128,256]{0,1:T(8,128)(2,1)}, bf16[128,256]{0,1:T(8,128)(2,1)}, u32[]{:S(2)}, u32[]{:S(2)}) collective-permute-start(bf16[128,256]{0,1:T(8,128)(2,1)} %get-tuple-element.13), channel_id=1, source_target_pairs={{0,8},{8,16},{16,24},{24,32},{32,40},{40,48},{48,56},{56,64},{64,7... | collective-permute-start | bytes 196616 | tf_op jit(solution)/shard_map/ppermute | solution.py:44
  63.2 4.8 %collective-permute-start.1 = (bf16[128,256]{0,1:T(8,128)(2,1)}, bf16[128,256]{0,1:T(8,128)(2,1)}, u32[]{:S(2)}, u32[]{:S(2)}) collective-permute-start(bf16[128,256]{0,1:T(8,128)(2,1)} %get-tuple-element.14), channel_id=1, source_target_pairs={{8,0},{16,8},{24,16},{32,24},{40,32},{48,40},{56,48},{64,56},{72,6... | collective-permute-start | bytes 196616 | tf_op jit(solution)/shard_map/ppermute | solution.py:45
  68.0 2.6 %multiply_reduce_fusion = (f32[1024,4]{0,1:T(4,128)S(1)}, f32[1024,4,128]{0,2,1:T(8,128)S(1)}) fusion(bf16[4,128,2048]{2,1,0:T(8,128)(2,1)S(1)} %bitcast.187, bf16[1,1024,2048]{2,1,0:T(8,128)(2,1)S(1)} %copy-done.1, f32[2048]{0:T(1024)S(1)} %bitcast.203, f32[2048]{0:T(1024)S(1)} %bitcast.206, f32[2048]{0:T(1024)S(1)} %copy-done.14, ...), kind=kOutput, calls=%fused_computation.40 | convolution fusion | flops 2161111040 | bytes 8433664 | tf_op jit(solution)/shard_map/dot_general | solution.py:148
  71.6 1.1 subtract_convert_fusion.1
  72.7 1.0 copy.78
  73.7 1.7 copy.85
  75.4 0.7 copy.86
  76.2 0.8 copy.84
  76.9 0.7 copy.83
  77.7 2.3 %copy.61 = bf16[8,128,4,32]{3,1,2,0:T(8,128)(2,1)} copy(bf16[8,128,4,32]{1,0,3,2:T(8,128)(2,1)} %bitcast.194) | data formatting | bytes 524288 | tf_op jit(solution)/shard_map/concatenate | solution.py:98
  80.0 2.3 %copy.62 = bf16[8,128,4,32]{3,1,2,0:T(8,128)(2,1)} copy(bf16[8,128,4,32]{1,0,3,2:T(8,128)(2,1)} %bitcast.193) | data formatting | bytes 524288 | tf_op jit(solution)/shard_map/concatenate | solution.py:98
  82.3 2.3 %copy.64 = bf16[8,128,4,32]{3,1,2,0:T(8,128)(2,1)} copy(bf16[8,128,4,32]{1,0,3,2:T(8,128)(2,1)} %bitcast.192) | data formatting | bytes 524288 | tf_op jit(solution)/shard_map/concatenate | solution.py:98
  84.6 2.3 %copy.63 = bf16[8,128,4,32]{3,1,2,0:T(8,128)(2,1)} copy(bf16[8,128,4,32]{1,0,3,2:T(8,128)(2,1)} %bitcast.191) | data formatting | bytes 524288 | tf_op jit(solution)/shard_map/concatenate | solution.py:98
  87.0 1.9 %pad_maximum_fusion.2 = (bf16[1024,256]{0,1:T(8,128)(2,1)}, bf16[1024,256]{0,1:T(8,128)(2,1)}) fusion(bf16[1024,256]{0,1:T(8,128)(2,1)S(1)} %fusion.35, bf16[128,256]{0,1:T(8,128)(2,1)} %collective-permute-done, bf16[128,256]{0,1:T(8,128)(2,1)} %collective-permute-done.1), kind=kLoop, calls=%fused_computation.66 | loop fusion | flops 2097152 | bytes 1703936 | tf_op jit(solution)/shard_map/concatenate | solution.py:46
  88.9 1.2 copy.77
  90.1 2.0 %copy.79 = bf16[1024,256]{1,0:T(8,128)(2,1)} copy(bf16[1024,256]{0,1:T(8,128)(2,1)} %get-tuple-element.12) | data formatting | bytes 1048576 | tf_op jit(solution)/shard_map/slice | solution.py:188
  92.2 1.3 pad_maximum_fusion
  93.5 1.2 copy-done.4
  94.7 7.4 %fusion.16 = (f32[4,8,128]{2,0,1:T(4,128)S(1)}, f32[8,384,128,4]{2,1,3,0:T(8,128)}) fusion(pred[8,128,384]{1,2,0:T(8,128)(4,1)} %broadcast_and_fusion, bf16[8,128,4,32]{3,1,2,0:T(8,128)(2,1)} %copy.64, bf16[8,128,4,32]{3,1,2,0:T(8,128)(2,1)} %copy.63, bf16[8,128,4,32]{3,1,2,0:T(8,128)(2,1)} %copy.62, bf16[8,128,4,32]{3,1,2,0:T(8,128)(2,1)} %copy.61, ...), kind=kOutput, calls=%fused_computation.23 | convolution fusion | flops 411561984 | bytes 8536064 | tf_op jit(solution)/shard_map/nqhgd,nkhd->hgnqk/dot_general | solution.py:209
  102.1 6.9 %bitcast_reduce_fusion = (f32[4,1024]{1,0:T(4,128)S(1)}, f32[768,1024,4]{1,0,2:T(8,128)}) fusion(bf16[1024,4,32]{0,2,1:T(8,128)(2,1)S(1)} %get-tuple-element.9, bf16[1024,4,32]{0,2,1:T(8,128)(2,1)S(1)} %copy-done.2, bf16[1024,4,32]{0,2,1:T(8,128)(2,1)S(1)} %get-tuple-element.6, bf16[1024,4,32]{0,2,1:T(8,128)(2,1)S(1)} %get-tuple-element.5, ...), kind=kOutput, calls=%fused_computation.1 | convolution fusion | flops 815788032 | bytes 13844480 | tf_op jit(solution)/shard_map/thgd,chd->hgtc/dot_general | solution.py:217
  109.1 2.0 %fusion.30 = f32[8,128,1,4,128]{4,1,3,0,2:T(8,128)S(1)} fusion(f32[4,8,128]{2,0,1:T(4,128)S(1)} %fusion.80, f32[8,384,128,4]{2,1,3,0:T(8,128)S(1)} %copy-done.18, pred[8,128,384]{1,2,0:T(8,128)(4,1)S(1)} %copy-done.13, bf16[8,384,256]{2,1,0:T(8,128)(2,1)S(1)} %copy-done.5), kind=kOutput, calls=%fused_computation.41 | convolution fusion | flops 408944640 | bytes 9584640 | tf_op jit(solution)/shard_map/hgnqk,nkhd->nqhgd/dot_general | solution.py:230
  111.2 1.4 copy.67
  112.6 2.9 %copy.70 = f32[1024,1,4,128]{0,3,2,1:T(8,128)} copy(f32[1024,1,4,128]{3,0,2,1:T(8,128)} %bitcast.180) | data formatting | bytes 4194304 | tf_op jit(solution)/shard_map/reshape | solution.py:236
  115.5 7.7 %fusion.27 = bf16[1024,1,4,128]{0,3,2,1:T(8,128)(2,1)S(1)} fusion(f32[1024,1,4,128]{0,3,2,1:T(8,128)} %copy.70, f32[4,1024]{1,0:T(4,128)S(1)} %fusion.79, f32[768,1024,4]{1,0,2:T(8,128)} %get-tuple-element.35, bf16[768,256]{1,0:T(8,128)(2,1)} %bitcast.31), kind=kOutput, calls=%fused_computation.35 | convolution fusion | flops 815792128 | bytes 15941632 | tf_op jit(solution)/shard_map/hgtc,chd->thgd/dot_general | solution.py:233
  123.3 4.4 %convolution_convert_fusion = bf16[1024,2048]{1,0:T(8,128)(2,1)} fusion(bf16[1024,512]{0,1:T(8,128)(2,1)S(1)} %bitcast.208, bf16[512,2048]{1,0:T(8,128)(2,1)S(1)} %copy-done), kind=kOutput, calls=%fused_computation.30 | convolution fusion | flops 2149580800 | bytes 7340032 | tf_op jit(solution)/shard_map/dot_general | solution.py:242
  127.6 4.8 %all-to-all-start.3 = ((bf16[4,256,2048]{2,1,0:T(8,128)(2,1)}), bf16[4,256,2048]{2,1,0:T(8,128)(2,1)}, u32[]{:S(2)}, u32[]{:S(2)}) async-start(bf16[4,256,2048]{2,1,0:T(8,128)(2,1)} %bitcast.181), calls=%async_computation.3 | async-start | bytes 8388608 | tf_op jit(solution)/shard_map/all_to_all | solution.py:57
  132.5 45.7 %all-to-all-done.3 = bf16[4,256,2048]{2,1,0:T(8,128)(2,1)} async-done(((bf16[4,256,2048]{2,1,0:T(8,128)(2,1)}), bf16[4,256,2048]{2,1,0:T(8,128)(2,1)}, u32[]{:S(2)}, u32[]{:S(2)}) %all-to-all-start.3) | async-done | bytes 4194336 | tf_op jit(solution)/shard_map/all_to_all | solution.py:57
  178.2 3.3 %convert_reduce_fusion = f32[256,2048]{1,0:T(8,128)S(1)} fusion(bf16[4,256,2048]{2,1,0:T(8,128)(2,1)} %all-to-all-done.3), kind=kLoop, calls=%fused_computation.17 | loop fusion | flops 3670016 | bytes 6291456 | tf_op jit(solution)/shard_map/reduce_sum | solution.py:58
  181.5 2.6 %fusion.29 = bf16[1,256,2048]{2,1,0:T(8,128)(2,1)} fusion(f32[256,2048]{1,0:T(8,128)S(1)} %convert_reduce_fusion, f32[2048]{0:T(1024)S(1)} %bitcast.200, bf16[1,1024,2048]{2,1,0:T(8,128)(2,1)} %param.15, s32[]{:T(128)S(6)} %select_n.33), kind=kLoop, calls=%fused_computation.38 | loop fusion | flops 2097152 | bytes 4202500 | tf_op jit(solution)/shard_map/convert_element_type | solution.py:247
  (67 shorter events, 4.6 us)
Async XLA Ops:
  0.0 123.3 %copy-start = (bf16[512,2048]{1,0:T(8,128)(2,1)S(1)}, bf16[512,2048]{1,0:T(8,128)(2,1)}, u32[]{:S(2)}) copy-start(bf16[512,2048]{1,0:T(8,128)(2,1)} %param.26) | copy-start | bytes 6291460
  0.0 19.4 %copy-start.6 = (bf16[1,24,2048]{2,1,0:T(8,128)(2,1)S(1)}, bf16[1,24,2048]{2,1,0:T(8,128)(2,1)}, u32[]{:S(2)}) copy-start(bf16[1,24,2048]{2,1,0:T(8,128)(2,1)} %param.16) | copy-start | bytes 294916
  0.0 38.3 %copy-start.17 = (f32[4]{0:T(128)S(1)}, f32[4]{0:T(128)}, u32[]{:S(2)}) copy-start(f32[4]{0:T(128)} %param.29) | copy-start | bytes 52
  4.7 28.6 %all-to-all-start = ((f32[32,5,512]{2,1,0:T(8,128)}), f32[32,5,512]{2,1,0:T(8,128)S(1)}, u32[]{:S(2)}, u32[]{:S(2)}) async-start(f32[32,5,512]{2,1,0:T(8,128)} %broadcast_in_dim.14), calls=%async_computation | async-start | bytes 1048576 | tf_op jit(solution)/shard_map/all_to_all | solution.py:17
  16.2 27.7 %copy-start.14 = (f32[2048]{0:T(1024)S(1)}, f32[2048]{0:T(1024)}, u32[]{:S(2)}) copy-start(f32[2048]{0:T(1024)} %param.19) | copy-start | bytes 24580
  19.3 24.9 %copy-start.10 = (bf16[2048,128]{1,0:T(8,128)(2,1)S(1)}, bf16[2048,128]{1,0:T(8,128)(2,1)}, u32[]{:S(2)}) copy-start(bf16[2048,128]{1,0:T(8,128)(2,1)} %param.24) | copy-start | bytes 1572868
  19.3 25.3 %copy-start.15 = (f32[128]{0:T(128)S(1)}, f32[128]{0:T(128)}, u32[]{:S(2)}) copy-start(f32[128]{0:T(128)} %param.28) | copy-start | bytes 1540
  33.3 10.6 %copy-start.11 = (bf16[2048,128]{1,0:T(8,128)(2,1)S(1)}, bf16[2048,128]{1,0:T(8,128)(2,1)}, u32[]{:S(2)}) copy-start(bf16[2048,128]{1,0:T(8,128)(2,1)} %param.25) | copy-start | bytes 1572868
  34.0 9.9 %all-to-all-start.1 = ((f32[4,5,512]{2,1,0:T(8,128)}), f32[4,5,512]{2,1,0:T(8,128)S(1)}, u32[]{:S(2)}, u32[]{:S(2)}) async-start(f32[4,5,512]{2,1,0:T(8,128)} %broadcast_in_dim.15), calls=%async_computation.1 | async-start | bytes 131072 | tf_op jit(solution)/shard_map/all_to_all | solution.py:17
  45.5 56.6 %all-to-all-start.2 = ((bf16[32,24,256]{2,1,0:T(8,128)(2,1)}), bf16[32,24,256]{2,1,0:T(8,128)(2,1)}, u32[]{:S(2)}, u32[]{:S(2)}) async-start(bf16[32,24,256]{2,1,0:T(8,128)(2,1)} %broadcast_in_dim.18), calls=%async_computation.2 | async-start | bytes 786432 | tf_op jit(solution)/shard_map/all_to_all | solution.py:17
  50.7 6.5 %copy-start.1 = (bf16[1,1024,2048]{2,1,0:T(8,128)(2,1)S(1)}, bf16[1,1024,2048]{2,1,0:T(8,128)(2,1)}, u32[]{:S(2)}) copy-start(bf16[1,1024,2048]{2,1,0:T(8,128)(2,1)} %param.15) | copy-start | bytes 12582916
  50.7 6.5 %copy-start.12 = (bf16[2048,128]{1,0:T(8,128)(2,1)S(1)}, bf16[2048,128]{1,0:T(8,128)(2,1)}, u32[]{:S(2)}) copy-start(bf16[2048,128]{1,0:T(8,128)(2,1)} %param.25) | copy-start | bytes 1572868
  57.3 10.7 %copy-start.3 = (bf16[512,2048]{1,0:T(8,128)(2,1)S(1)}, bf16[512,2048]{1,0:T(8,128)(2,1)}, u32[]{:S(2)}) copy-start(bf16[512,2048]{1,0:T(8,128)(2,1)} %copy.80) | copy-start | bytes 6291460
  59.8 27.1 %collective-permute-start = (bf16[128,256]{0,1:T(8,128)(2,1)}, bf16[128,256]{0,1:T(8,128)(2,1)}, u32[]{:S(2)}, u32[]{:S(2)}) collective-permute-start(bf16[128,256]{0,1:T(8,128)(2,1)} %get-tuple-element.13), channel_id=1, source_target_pairs={{0,8},{8,16},{16,24},{24,32},{32,40},{40,48},{48,56},{56,64},{64,7... | collective-permute-start | bytes 196616 | tf_op jit(solution)/shard_map/ppermute | solution.py:44
  63.2 23.8 %collective-permute-start.1 = (bf16[128,256]{0,1:T(8,128)(2,1)}, bf16[128,256]{0,1:T(8,128)(2,1)}, u32[]{:S(2)}, u32[]{:S(2)}) collective-permute-start(bf16[128,256]{0,1:T(8,128)(2,1)} %get-tuple-element.14), channel_id=1, source_target_pairs={{8,0},{16,8},{24,16},{32,24},{40,32},{48,40},{56,48},{64,56},{72,6... | collective-permute-start | bytes 196616 | tf_op jit(solution)/shard_map/ppermute | solution.py:45
  68.0 2.7 %copy-start.16 = (f32[128]{0:T(128)S(1)}, f32[128]{0:T(128)}, u32[]{:S(2)}) copy-start(f32[128]{0:T(128)} %param.27) | copy-start | bytes 1540
  70.6 0.9 copy-start.7
  70.6 1.0 copy-start.8
  70.6 1.0 copy-start.9
  93.5 1.2 copy-start.4
  94.7 7.4 %copy-start.2 = (bf16[1024,4,32]{0,2,1:T(8,128)(2,1)S(1)}, bf16[1024,4,32]{0,2,1:T(8,128)(2,1)}, u32[]{:S(2)}) copy-start(bf16[1024,4,32]{0,2,1:T(8,128)(2,1)} %get-tuple-element.10) | copy-start | bytes 786436
  102.1 7.0 %copy-start.5 = (bf16[8,384,256]{2,1,0:T(8,128)(2,1)S(1)}, bf16[8,384,256]{2,1,0:T(8,128)(2,1)}, u32[]{:S(2)}) copy-start(bf16[8,384,256]{2,1,0:T(8,128)(2,1)} %copy-done.4) | copy-start | bytes 4718596
  102.1 7.0 %copy-start.13 = (pred[8,128,384]{1,2,0:T(8,128)(4,1)S(1)}, pred[8,128,384]{1,2,0:T(8,128)(4,1)}, u32[]{:S(2)}) copy-start(pred[8,128,384]{1,2,0:T(8,128)(4,1)} %broadcast_and_fusion) | copy-start | bytes 1179652
  102.1 7.0 %copy-start.18 = (f32[8,384,128,4]{2,1,3,0:T(8,128)S(1)}, f32[8,384,128,4]{2,1,3,0:T(8,128)}, u32[]{:S(2)}) copy-start(f32[8,384,128,4]{2,1,3,0:T(8,128)} %get-tuple-element.31) | copy-start | bytes 18874372
  127.6 50.6 %all-to-all-start.3 = ((bf16[4,256,2048]{2,1,0:T(8,128)(2,1)}), bf16[4,256,2048]{2,1,0:T(8,128)(2,1)}, u32[]{:S(2)}, u32[]{:S(2)}) async-start(bf16[4,256,2048]{2,1,0:T(8,128)(2,1)} %bitcast.181), calls=%async_computation.3 | async-start | bytes 8388608 | tf_op jit(solution)/shard_map/all_to_all | solution.py:57
where the time goes:
time: 185 us; the launch traced here: 184 us
  waiting for transfers between devices  58.1 us (31%)
  matrix products  40.6 us (22%)
  starting transfers between devices  33.9 us (18%)
  local copies, waits for them, and re-layouts  30.6 us (17%)
  other arithmetic  20.5 us (11%)
    all_to_all x1, waiting for transfers between devices, summed_on_arrival(): pieces = lax.all_to_all(split_up(array, dim, peers), axis, 0, 0, tiled=True)  45.7 us
    all_to_all x3, starting transfers between devices, from_everyone(): lax.all_to_all(jnp.broadcast_to(array[None], (peers, *array.shape)), axis...  20.9 us
    all_to_all x3, waiting for transfers between devices, from_everyone(): lax.all_to_all(jnp.broadcast_to(array[None], (peers, *array.shape)), axis...  12.4 us
    concatenate x4, local copies, waits for them, and re-layouts, rotate(): jnp.concatenate([rotate_half(vectors[..., :half_dim], positions // GRID_W...  9.27 us
    dot_general x1, matrix products, per_device(): jnp.einsum('hgtc,chd->thgd', ctx_probs, ctx_values, preferred_element_typ...  7.74 us
    dot_general x1, matrix products, per_device(): jnp.einsum('nqhgd,nkhd->hgnqk', query_blocks, window_keys, preferred_elem...  7.4 us
    dot_general x1, matrix products, per_device(): jnp.einsum('thgd,chd->hgtc', flat_queries, ctx_keys, preferred_element_ty...  6.85 us
    unnamed x42, local copies, waits for them, and re-layouts  5.73 us
  transfers between devices with their start and end apart: 6, of which 3 were waited for; matrix products, arithmetic and copies ran while one was open for 28% of the time, Pallas kernels for 0%

commit v1 on v0

v1 whole, which is shorter than its diff:
```python
import functools
import math

import jax
import jax.numpy as jnp
import numpy as np
from jax import lax
from jax.experimental import pallas as pl
from jax.experimental.pallas import tpu as pltpu
from jax.sharding import PartitionSpec as P

HEAD_DIM = 128
WINDOW = 128
GRID_W = 64
NORM_EPSILON = 1e-06
ROPE_BASE = 10000.0

MESH = pl.DeviceIdType.MESH
F32 = jnp.float32
BF16 = jnp.bfloat16

NY, NZ, NX = 4, 8, 4
D = 2048
COLS = 512
TOK = 1024
SUB = TOK // NX
ROWS = 256
CROWS = 24
CTX = CROWS * NY * NZ
GROUP = 4
NBLK = TOK // WINDOW
Q_FOLD = HEAD_DIM ** (-0.5) * math.log2(math.e)


def rope_tables(n_sp):
    quarter = HEAD_DIM // 4
    freq = np.float32(ROPE_BASE) ** (-np.arange(quarter, dtype=np.float32) / np.float32(quarter))
    sign = np.concatenate([-np.ones(quarter), np.ones(quarter)]).astype(np.float32)

    def table(coords):
        angles = coords.astype(np.float32)[:, None] * freq[None, :].astype(np.float32)
        angles = np.concatenate([angles, angles], axis=1).astype(np.float64)
        return np.cos(angles).astype(np.float32), np.sin(angles).astype(np.float32) * sign

    row_count = n_sp * TOK // GRID_W
    rc, rs = table(np.arange(row_count))
    cc, cs = table(np.arange(GRID_W))
    rz, cz = np.zeros_like(rc), np.zeros_like(cc)
    rows = np.stack([np.concatenate([rc, rz], 1), np.concatenate([rs, rz], 1)])
    rows = rows.reshape(2, n_sp, TOK // GRID_W, HEAD_DIM).transpose(1, 0, 2, 3)
    cols = np.stack([np.concatenate([cz, cc], 1), np.concatenate([cz, cs], 1)])
    return np.ascontiguousarray(rows), cols


def swap_quarters(v):
    lane = lax.broadcasted_iota(jnp.int32, v.shape, v.ndim - 1)
    even = (lane // 32) % 2 == 0
    return jnp.where(even, pltpu.roll(v, 96, v.ndim - 1), pltpu.roll(v, 32, v.ndim - 1))


def kernel(
    lat_h, ctx_h, cond_h, cctx_h, gain_h, msh_h, msc_h, mga_h, wq_h, wk_h, wv_h, wo_h,
    qg_h, kg_h, sink_h, rowt_h, colt_h, out_h,
    lat, ctx, cnd, gain, modw, wqkv, wo, hg, sink, rowt, colt,
    pm, ym, zs, zm, xm, vec, rinv, lin, cin, tab, qb, kvb, cpiece, cz, ckv, acc, att, attx, res,
    ld, y_s, y_r, z_s, z_r, x_s, x_r, cz_s, cz_r, cy_s, cy_r, h_s, h_r, a_s, a_r,
    s_s, s_r, r_s, r_r, w_s, w_r, d_s, d_r, o_s,
):
    sp = lax.axis_index("sp")
    tp = lax.axis_index("tp")
    dp = lax.axis_index("dp")
    y = lax.rem(sp, NY)
    z = sp // NY
    n_sp = NY * NZ

    def y_peer(d):
        return {"sp": z * NY + lax.rem(y + d, NY)}

    def z_peer(d):
        return {"sp": lax.rem(z + d, NZ) * NY + y}

    def x_peer(d):
        return {"tp": lax.rem(tp + d, NX)}

    partner = {"dp": 1 - dp}
    right = {"sp": lax.rem(sp + 1, n_sp)}
    left = {"sp": lax.rem(sp + n_sp - 1, n_sp)}

    def remote(src, dst, send, recv, dev):
        return pltpu.make_async_remote_copy(
            src_ref=src, dst_ref=dst, send_sem=send, recv_sem=recv, device_id=dev, device_id_type=MESH
        )

    def load(src, dst, k):
        c = pltpu.make_async_copy(src, dst, ld.at[k])
        c.start()
        return c

    barrier = pltpu.get_barrier_semaphore()
    peers = [y_peer(d) for d in range(1, NY)] + [z_peer(d) for d in range(1, NZ)]
    peers += [x_peer(d) for d in range(1, NX)] + [partner, left, right]
    for dev in peers:
        pl.semaphore_signal(barrier, inc=1, device_id=dev, device_id_type=MESH)

    l_mod = [
        load(msh_h, modw.at[0], 0),
        load(msc_h, modw.at[1], 1),
        load(mga_h, modw.at[2], 2),
        load(cond_h, cnd.at[pl.ds(0, 1), :], 3),
        load(cctx_h, cnd.at[pl.ds(1, 1), :], 4),
    ]
    l_lat = [
        load(lat_h.at[pl.ds(i * 256, 256), :], lat.at[pl.ds(i * 256, 256), :], 5 + i) for i in range(4)
    ]
    l_small = [
        load(gain_h, gain, 9),
        load(qg_h, hg.at[pl.ds(0, 1), :], 10),
        load(kg_h, hg.at[pl.ds(1, 1), :], 11),
        load(sink_h, sink, 12),
        load(rowt_h.at[sp], rowt, 13),
        load(colt_h, colt, 14),
        load(ctx_h, ctx, 15),
    ]
    l_kv = [
        load(wk_h, wqkv.at[:, pl.ds(COLS, HEAD_DIM)], 16),
        load(wv_h, wqkv.at[:, pl.ds(COLS + HEAD_DIM, HEAD_DIM)], 17),
    ]
    l_q = load(wq_h, wqkv.at[:, pl.ds(0, COLS)], 18)
    l_wo = load(wo_h, wo.at[pl.ds(pl.multiple_of(tp * COLS, COLS), COLS), :], 19)

    for c in l_mod:
        c.wait()
    half = cnd[:, pl.ds(pl.multiple_of((sp // 2) * 128, 128), 128)]
    act = half / (1.0 + jnp.exp(-half))
    flipped = jnp.concatenate([act[:, 64:], act[:, :64]], axis=1)
    act = jnp.where(lax.rem(sp, 2) == 1, flipped, act)[:, :64].astype(BF16)
    pm[...] = jnp.zeros_like(pm)
    for k in range(3):
        pm[pl.ds(2 * k, 2), :] = jnp.dot(act, modw[k], preferred_element_type=F32)

    pl.semaphore_wait(barrier, len(peers))

    y_cp = [remote(pm, ym.at[d - 1], y_s.at[d - 1], y_r.at[d - 1], y_peer(d)) for d in range(1, NY)]
    for c in y_cp:
        c.start()

    color = lax.rem(y, 2)
    quarter = 2 * color + dp
    other = 2 * (1 - color) + dp
    x_before = lax.rem(tp + 3, NX)
    x_after = lax.rem(tp + 1, NX)
    x_far = lax.rem(tp + 2, NX)

    def wo_rows(block, q, chunk, count):
        return wo.at[pl.ds(pl.multiple_of(block * COLS + q * 128 + chunk * 64, 64), count), :]

    def own_rows(chunk):
        return wo_h.at[pl.ds(pl.multiple_of(quarter * 128 + chunk * 64, 64), 64), :]

    s_cp = [
        [
            remote(own_rows(c), wo_rows(tp, quarter, c, 64), s_s.at[2 * k + c], s_r.at[2 * k + c], x_peer(step))
            for c in range(2)
        ]
        for k, step in enumerate((1, 3))
    ]
    for k in range(2):
        s_cp[k][0].start()

    def norms(i, carry):
        rows = pl.ds(pl.multiple_of(i * 64, 64), 64)
        total = jnp.zeros((64, 128), F32)
        for c in range(D // 128):
            v = lat[rows, pl.ds(c * 128, 128)].astype(F32)
            total = total + v * v
        mean = jnp.sum(total, axis=-1, keepdims=True) * (1.0 / D)
        rinv[rows, :] = jnp.broadcast_to(lax.rsqrt(mean + NORM_EPSILON), (64, 128))
        return carry

    for c in l_lat[:2]:
        c.wait()
    lax.fori_loop(0, 4, norms, 0)

    for c in y_cp:
        c.wait_recv()
    zs[...] = (pm[...] + ym[0]) + (ym[1] + ym[2])
    z_cp = [remote(zs, zm.at[d - 1], z_s.at[d - 1], z_r.at[d - 1], z_peer(d)) for d in range(1, NZ)]
    for c in z_cp:
        c.start()

    for c in l_lat[2:]:
        c.wait()
    lax.fori_loop(4, 16, norms, 0)

    for c in z_cp:
        c.wait_recv()
    xm[tp] = (zs[...] + zm[0]) + (zm[1] + zm[2]) + ((zm[3] + zm[4]) + (zm[5] + zm[6]))
    x_cp = [remote(xm.at[tp], xm.at[tp], x_s.at[d - 1], x_r.at[d - 1], x_peer(d)) for d in range(1, NX)]
    for c in x_cp:
        c.start()
    for k in range(2):
        s_cp[k][1].start()

    for c in l_small + l_kv:
        c.wait()
    c_total = jnp.zeros((CROWS, 128), F32)
    for c in range(D // 128):
        v = ctx[:, pl.ds(c * 128, 128)].astype(F32)
        c_total = c_total + v * v
    c_mean = jnp.sum(c_total, axis=-1, keepdims=True) * (1.0 / D)
    c_inv = jnp.broadcast_to(lax.rsqrt(c_mean + NORM_EPSILON), (CROWS, 128))

    for d in range(1, NX):
        remote(
            xm.at[tp], xm.at[lax.rem(tp + NX - d, NX)], x_s.at[d - 1], x_r.at[d - 1], x_peer(d)
        ).wait_recv()
    for j in range(NX):
        cols = pl.ds(j * COLS, COLS)
        g = gain[:, cols]
        for k, row in ((0, g * (1.0 + xm[j, 2:3, :])), (1, xm[j, 0:1, :]), (2, g * (1.0 + xm[j, 3:4, :])),
                       (3, xm[j, 1:2, :]), (4, xm[j, 4:5, :])):
            vec[k, :, cols] = jnp.broadcast_to(row, (8, COLS))

    for c in range(D // 128):
        cols = pl.ds(c * 128, 128)
        v = ctx[:, cols].astype(F32) * c_inv
        v = v.reshape(CROWS // 8, 8, 128) * vec[2, :, cols][None] + vec[3, :, cols][None]
        cin[:, cols] = v.reshape(CROWS, 128).astype(BF16)
    kv = jnp.dot(cin[...], wqkv[:, pl.ds(COLS, 2 * HEAD_DIM)], preferred_element_type=F32)
    key = kv[:, :HEAD_DIM]
    mean = jnp.mean(key * key, axis=-1, keepdims=True)
    key = key * lax.rsqrt(mean + NORM_EPSILON) * hg[1:2, :]
    cpiece[:, pl.ds(0, HEAD_DIM)] = key.astype(BF16)
    cpiece[:, pl.ds(HEAD_DIM, HEAD_DIM)] = kv[:, HEAD_DIM:].astype(BF16)
    cz_cp = [
        remote(cpiece, cz.at[d - 1], cz_s.at[d - 1], cz_r.at[d - 1], z_peer(d)) for d in range(1, NZ)
    ]
    for c in cz_cp:
        c.start()

    l_q.wait()
    q_gain = jnp.broadcast_to(hg[0:1, :], (8, 128)) * Q_FOLD
    k_gain = jnp.broadcast_to(hg[1:2, :], (8, 128))
    q_swap, k_swap = swap_quarters(q_gain), swap_quarters(k_gain)
    halo_to_left = remote(
        kvb.at[pl.ds(WINDOW, WINDOW), :], kvb.at[pl.ds(TOK + WINDOW, WINDOW), :], h_s.at[0], h_r.at[0], left
    )
    halo_to_right = remote(
        kvb.at[pl.ds(TOK, WINDOW), :], kvb.at[pl.ds(0, WINDOW), :], h_s.at[1], h_r.at[1], right
    )

    def project(i, carry):
        b = lax.rem(3 * i, 4)
        base = pl.multiple_of(b * ROWS, ROWS)

        def modulate(r, c2):
            rows = pl.ds(pl.multiple_of(base + r * 64, 64), 64)
            inv = rinv[rows, :]
            for c in range(D // 128):
                cols = pl.ds(c * 128, 128)
                v = lat[rows, cols].astype(F32) * inv
                v = v.reshape(8, 8, 128) * vec[0, :, cols][None] + vec[1, :, cols][None]
                lin[pl.ds(pl.multiple_of(r * 64, 64), 64), cols] = v.reshape(64, 128).astype(BF16)
            return c2

        lax.fori_loop(0, ROWS // 64, modulate, 0)

        for g in range(ROWS // GRID_W):
            at = pl.ds(g * GRID_W, GRID_W)
            row = b * (ROWS // GRID_W) + g
            cosine = colt[0].reshape(8, 8, 128) + rowt[0, pl.ds(row, 1), :][None]
            sine = colt[1].reshape(8, 8, 128) + rowt[1, pl.ds(row, 1), :][None]
            tab[0, at, :] = (cosine * q_gain[None]).reshape(64, 128)
            tab[1, at, :] = (sine * q_swap[None]).reshape(64, 128)
            tab[2, at, :] = (cosine * k_gain[None]).reshape(64, 128)
            tab[3, at, :] = (sine * k_swap[None]).reshape(64, 128)

        def turned(v, t):
            inv = lax.rsqrt(jnp.mean(v * v, axis=-1, keepdims=True) + NORM_EPSILON)
            return ((v * tab[t] + swap_quarters(v) * tab[t + 1]) * inv).astype(BF16)

        for n in range(3):
            out = jnp.dot(lin[...], wqkv[:, pl.ds(n * 256, 256)], preferred_element_type=F32)
            first, second = out[:, :128], out[:, 128:]
            if n < 2:
                for h, v in ((2 * n, first), (2 * n + 1, second)):
                    t = turned(v, 0)
                    qb[2 * b, pl.ds(h * 128, 128), :] = t[:128]
                    qb[2 * b + 1, pl.ds(h * 128, 128), :] = t[128:]
            else:
                rows = pl.ds(pl.multiple_of(WINDOW + base, 128), ROWS)
                kvb[rows, pl.ds(0, 128)] = turned(first, 2)
                kvb[rows, pl.ds(128, 128)] = second.astype(BF16)

        @pl.when(i == 1)
        def _():
            halo_to_left.start()
            halo_to_right.start()

        return carry

    lax.fori_loop(0, TOK // ROWS, project, 0)

    def to_y(n, block):
        return [
            remote(
                wo_rows(block, quarter, c, 64), wo_rows(block, quarter, c, 64),
                w_s.at[2 * n + c], w_r.at[2 * n + c], y_peer((1, 3)[c]),
            )
            for c in range(2)
        ]

    def from_y(n, block):
        return [
            remote(
                wo_rows(block, other, c, 64), wo_rows(block, other, c, 64),
                w_s.at[2 * n + c], w_r.at[2 * n + c], y_peer((1, 3)[c]),
            )
            for c in range(2)
        ]

    def to_partner(n, block, q):
        rows = wo_rows(block, q, 0, 128)
        return remote(rows, rows, d_s.at[n], d_r.at[n], partner)

    for k, block in enumerate((x_before, x_after)):
        for c in range(2):
            remote(
                own_rows(c), wo_rows(block, quarter, c, 64), s_s.at[2 * k + c], s_r.at[2 * k + c],
                x_peer((1, 3)[k]),
            ).wait_recv()
    r_cp = [
        remote(
            wo_rows(block, quarter, k, 64), wo_rows(block, quarter, k, 64), r_s.at[k], r_r.at[k],
            x_peer((1, 3)[k]),
        )
        for k, block in enumerate((x_before, x_after))
    ]
    for c in r_cp:
        c.start()
    y_w = [to_y(n, block) for n, block in enumerate((x_before, x_after))]
    d_w = [to_partner(n, block, quarter) for n, block in enumerate((x_before, x_after))]
    for n in range(2):
        for c in y_w[n]:
            c.start()
        d_w[n].start()

    for c in cz_cp:
        c.wait_recv()
    pieces = [cpiece[...].astype(F32)] + [cz[d].astype(F32) for d in range(NZ - 1)]
    ckv[pl.ds(0, CROWS * NZ), :] = jnp.concatenate(pieces, axis=0).astype(BF16)
    zrows = CROWS * NZ
    cy_cp = [
        remote(
            ckv.at[pl.ds(0, zrows), :], ckv.at[pl.ds(d * zrows, zrows), :], cy_s.at[d - 1], cy_r.at[d - 1],
            y_peer(d),
        )
        for d in range(1, NY)
    ]
    for c in cy_cp:
        c.start()

    halo_to_left.wait_recv()
    halo_to_right.wait_recv()
    stacked = GROUP * WINDOW
    q_row = lax.rem(lax.broadcasted_iota(jnp.int32, (stacked, WINDOW), 0), WINDOW)
    k_row = lax.broadcasted_iota(jnp.int32, (stacked, WINDOW), 1)
    ahead = k_row - q_row

    def window(i, carry):
        b = lax.rem(i + 1, NBLK)
        rows = pl.ds(pl.multiple_of(b * WINDOW, WINDOW), 3 * WINDOW)
        k = kvb[rows, pl.ds(0, 128)]
        v = kvb[rows, pl.ds(128, 128)]
        s = lax.dot_general(qb[b], k, (((1,), (1,)), ((), ())), preferred_element_type=F32)
        e = jnp.exp2(s)
        no_left = jnp.logical_and(sp == 0, b == 0).astype(jnp.int32) * (2 * WINDOW)
        no_right = jnp.logical_and(sp == n_sp - 1, b == NBLK - 1).astype(jnp.int32) * (2 * WINDOW)
        e_left = jnp.where(ahead >= no_left, e[:, :WINDOW], 0.0)
        e_right = jnp.where(ahead <= -no_right, e[:, 2 * WINDOW :], 0.0)
        p = jnp.concatenate([e_left, e[:, WINDOW : 2 * WINDOW], e_right], axis=1).astype(BF16)
        v2 = jnp.concatenate([v, jnp.ones((3 * WINDOW, 128), BF16)], axis=1)
        acc[b] = jnp.dot(p, v2, preferred_element_type=F32)
        return carry

    lax.fori_loop(0, NBLK, window, 0)

    for k in range(2):
        remote(
            wo_rows(x_far, quarter, k, 64), wo_rows(x_far, quarter, k, 64), r_s.at[k], r_r.at[k],
            x_peer((1, 3)[k]),
        ).wait_recv()
    y_w.append(to_y(2, x_far))
    d_w.append(to_partner(2, x_far, quarter))
    for c in y_w[2]:
        c.start()
    d_w[2].start()

    for c in cy_cp:
        c.wait_recv()

    def att_rows(i):
        return pl.ds(pl.multiple_of(lax.rem(i, 2) * WINDOW, WINDOW), WINDOW)

    my_cols = pl.ds(pl.multiple_of(tp * COLS, COLS), COLS)

    def context_part(i, carry):
        dist = lax.rem(i // 2 + 1, NX)
        dest = lax.rem(tp + dist, NX)
        b = 2 * dest + lax.rem(i, 2)
        k = ckv[:, pl.ds(0, 128)]
        v = ckv[:, pl.ds(128, 128)]
        s = lax.dot_general(qb[b], k, (((1,), (1,)), ((), ())), preferred_element_type=F32)
        p = jnp.exp2(s).astype(BF16)
        v2 = jnp.concatenate([v, jnp.ones((CTX, 128), BF16)], axis=1)
        o = acc[b] + jnp.dot(p, v2, preferred_element_type=F32)
        for h in range(GROUP):
            at = slice(h * WINDOW, (h + 1) * WINDOW)
            sink_exp = jnp.broadcast_to(jnp.exp(sink[:, h : h + 1]), (WINDOW, 128))
            att[i, :, pl.ds(h * 128, 128)] = (o[at, :128] / (o[at, 128:] + sink_exp)).astype(BF16)

        @pl.when(i < 6)
        def _():
            remote(att.at[i], attx.at[att_rows(i), my_cols], a_s.at[i], a_r.at[i], {"tp": dest}).start()

        @pl.when(i >= 6)
        def _():
            attx[att_rows(i), my_cols] = att[i]

        return carry

    lax.fori_loop(0, NBLK, context_part, 0)

    for n, block in enumerate((x_before, x_after, x_far)):
        for c in from_y(n, block):
            c.wait_recv()
    d2_w = [to_partner(3 + n, block, other) for n, block in enumerate((x_before, x_after, x_far))]
    for c in d2_w:
        c.start()

    a_cp = []
    for i in range(6):
        dist = i // 2 + 1
        src = lax.rem(tp + NX - dist, NX)
        cols = pl.ds(pl.multiple_of(src * COLS, COLS), COLS)
        c = remote(
            att.at[i], attx.at[pl.ds((i % 2) * WINDOW, WINDOW), cols], a_s.at[i], a_r.at[i],
            {"tp": lax.rem(tp + dist, NX)},
        )
        c.wait_recv()
        a_cp.append(c)
    p_quarter, p_other = 2 * color + 1 - dp, 2 * (1 - color) + 1 - dp
    for n, block in enumerate((x_before, x_after, x_far)):
        to_partner(n, block, p_quarter).wait_recv()
        to_partner(3 + n, block, p_other).wait_recv()
    l_wo.wait()

    def out_part(n, carry):
        cols = pl.ds(pl.multiple_of(n * 512, 512), 512)
        mixed = jnp.dot(attx[...], wo[:, cols], preferred_element_type=F32)
        own = lat[pl.ds(pl.multiple_of(tp * SUB, SUB), SUB), cols].astype(F32)
        mixed = mixed.reshape(SUB // 8, 8, 512) * vec[4, :, cols][None]
        res[:, cols] = (own + mixed.reshape(SUB, 512)).astype(BF16)
        pltpu.make_async_copy(res.at[:, cols], out_h.at[:, cols], o_s.at[n]).start()
        return carry

    lax.fori_loop(0, D // 512, out_part, 0)

    for c in y_cp + z_cp + x_cp + cz_cp + cy_cp + r_cp + d_w + d2_w + a_cp:
        c.wait_send()
    for group in s_cp + y_w:
        for c in group:
            c.wait_send()
    halo_to_left.wait_send()
    halo_to_right.wait_send()
    for n in range(D // 512):
        cols = pl.ds(n * 512, 512)
        pltpu.make_async_copy(res.at[:, cols], out_h.at[:, cols], o_s.at[n]).wait()


def per_device(*args):
    (latent, context, cond, ctx_cond, norm_gain, mod_shift, mod_scale, mod_gate, w_query, w_key, w_value, w_out,
     q_gain, k_gain, sinks) = args
    rows, cols = rope_tables(NY * NZ)
    operands = (
        latent[0], context[0], cond, ctx_cond.reshape(1, D), norm_gain.reshape(1, D), mod_shift, mod_scale,
        mod_gate, w_query, w_key, w_value, w_out, q_gain.reshape(1, HEAD_DIM), k_gain.reshape(1, HEAD_DIM),
        sinks.reshape(1, GROUP), jnp.asarray(rows), jnp.asarray(cols),
    )
    dma = pltpu.SemaphoreType.DMA
    vm = pltpu.VMEM
    scratch = [
        vm((TOK, D), BF16), vm((CROWS, D), BF16), vm((2, D), F32), vm((1, D), F32), vm((3, 64, COLS), BF16),
        vm((D, COLS + 2 * HEAD_DIM), BF16), vm((D, D), BF16), vm((2, HEAD_DIM), F32), vm((1, GROUP), F32),
        vm((2, TOK // GRID_W, HEAD_DIM), F32), vm((2, GRID_W, HEAD_DIM), F32),
        vm((8, COLS), F32), vm((3, 8, COLS), F32), vm((8, COLS), F32), vm((7, 8, COLS), F32),
        vm((NX, 8, COLS), F32), vm((5, 8, D), F32), vm((TOK, 128), F32), vm((ROWS, D), BF16), vm((CROWS, D), BF16),
        vm((4, ROWS, 128), F32), vm((NBLK, GROUP * WINDOW, 128), BF16), vm((TOK + 2 * WINDOW, 256), BF16),
        vm((CROWS, 256), BF16), vm((NZ - 1, CROWS, 256), BF16), vm((CTX, 256), BF16),
        vm((NBLK, GROUP * WINDOW, 256), F32), vm((NBLK, WINDOW, COLS), BF16), vm((SUB, D), BF16), vm((SUB, D), BF16),
        dma((20,)), dma((3,)), dma((3,)), dma((7,)), dma((7,)), dma((3,)), dma((3,)), dma((7,)), dma((7,)),
        dma((3,)), dma((3,)), dma((2,)), dma((2,)), dma((6,)), dma((6,)),
        dma((4,)), dma((4,)), dma((2,)), dma((2,)), dma((6,)), dma((6,)), dma((6,)), dma((6,)), dma((4,)),
    ]
    result = pl.pallas_call(
        kernel,
        out_shape=jax.ShapeDtypeStruct((SUB, D), BF16),
        in_specs=[pl.BlockSpec(memory_space=pl.ANY)] * len(operands),
        out_specs=pl.BlockSpec(memory_space=pl.ANY),
        scratch_shapes=scratch,
        compiler_params=pltpu.CompilerParams(
            collective_id=0, has_side_effects=True, vmem_limit_bytes=60 * 1024 * 1024
        ),
    )(*operands)
    return result[None]


def solution(mesh):
    in_specs = (
        P("dp", "sp", None), P("dp", "sp", None), P("dp", None), P(), P(), P("sp", "tp"), P("sp", "tp"),
        P("sp", "tp"), P(None, "tp"), P(None, "tp"), P(None, "tp"), P("tp", None), P(), P(), P("tp"),
    )
    out_specs = P("dp", ("sp", "tp"), None)
    return jax.shard_map(per_device, mesh=mesh, in_specs=in_specs, out_specs=out_specs, check_vma=False)
```

time: 185 us -> 66.2 us (0.36)
  the two profiles are of different devices: /device:TPU:32 before, /device:TPU:1 now
where the time goes in v1:
time: 66.2 us; the launch traced here: 66.1 us
  Pallas kernels  63.7 us (96%)
  local copies, waits for them, and re-layouts  2.3 us (3%)
    pallas_call x1, Pallas kernels, per_device(): pl.pallas_call(kernel, out_shape=jax.ShapeDtypeStruct((SUB, D), BF16), in...  63.7 us
    unnamed x1, local copies, waits for them, and re-layouts  2.3 us

profile of v1, /device:TPU:1, one launch (start us, length us, event | category | flops | bytes accessed | tf_op | source)
XLA Modules:
  0.0 66.1 jit_solution(10076830071970251743)
XLA Ops:
  0.0 63.7 %shard_map.163 = bf16[256,2048]{1,0:T(8,128)(2,1)} custom-call(bf16[1024,2048]{1,0:T(8,128)(2,1)} %bitcast.8, bf16[24,2048]{1,0:T(8,128)(2,1)} %bitcast.10, f32[1,2048]{1,0:T(1,128)} %cond_h.1, f32[1,2048]{1,0:T(1,128)} %bitcast.11, f32[1,2048]{1,0:T(1,128)} %bitcast.12, bf16[64,512]{1,0:T(8,128)(2,1)} %msh_h.1, bf16[64,512]{1,0:T(8,128)(2,1)} %msc_h.1, ...), custom_call_target="tpu_custom_call" | custom-call | tf_op jit(solution)/shard_map/pallas_call | solution.py:505
  63.7 2.3 %copy.19 = bf16[1,256,2048]{2,1,0:T(8,128)(2,1)} copy(bf16[1,256,2048]{2,1,0:T(8,128)(2,1)} %bitcast.9) | data formatting | bytes 2097152

commit v2 on v1

--- a/solution.py
+++ b/solution.py
@@ -62,7 +62,7 @@
     lat_h, ctx_h, cond_h, cctx_h, gain_h, msh_h, msc_h, mga_h, wq_h, wk_h, wv_h, wo_h,
     qg_h, kg_h, sink_h, rowt_h, colt_h, out_h,
     lat, ctx, cnd, gain, modw, wqkv, wo, hg, sink, rowt, colt,
-    pm, ym, zs, zm, xm, vec, rinv, lin, cin, tab, qb, kvb, cpiece, cz, ckv, acc, att, attx, res,
+    pm, ym, zs, zm, xm, vec, rinv, lin_a, lin_b, cin, tab, qb, kvb, cpiece, cz, ckv, acc, att, attx, mix, res,
     ld, y_s, y_r, z_s, z_r, x_s, x_r, cz_s, cz_r, cy_s, cy_r, h_s, h_r, a_s, a_r,
     s_s, s_r, r_s, r_r, w_s, w_r, d_s, d_r, o_s,
 ):
@@ -134,9 +134,10 @@
     act = half / (1.0 + jnp.exp(-half))
     flipped = jnp.concatenate([act[:, 64:], act[:, :64]], axis=1)
     act = jnp.where(lax.rem(sp, 2) == 1, flipped, act)[:, :64].astype(BF16)
-    pm[...] = jnp.zeros_like(pm)
-    for k in range(3):
-        pm[pl.ds(2 * k, 2), :] = jnp.dot(act, modw[k], preferred_element_type=F32)
+    part = jnp.concatenate(
+        [jnp.dot(act, modw[k], preferred_element_type=F32) for k in range(3)] + [jnp.zeros((2, COLS), F32)], axis=0
+    )
+    pm[...] = part.astype(BF16)
 
     pl.semaphore_wait(barrier, len(peers))
 
@@ -144,15 +145,15 @@
     for c in y_cp:
         c.start()
 
-    color = lax.rem(y, 2)
+    color = lax.rem(y + z, 2)
     quarter = 2 * color + dp
     other = 2 * (1 - color) + dp
     x_before = lax.rem(tp + 3, NX)
     x_after = lax.rem(tp + 1, NX)
     x_far = lax.rem(tp + 2, NX)
 
-    def wo_rows(block, q, chunk, count):
-        return wo.at[pl.ds(pl.multiple_of(block * COLS + q * 128 + chunk * 64, 64), count), :]
+    def wo_rows(block, q, chunk, count, extra=0):
+        return wo.at[pl.ds(pl.multiple_of(block * COLS + q * 128 + chunk * 64 + extra, 32), count), :]
 
     def own_rows(chunk):
         return wo_h.at[pl.ds(pl.multiple_of(quarter * 128 + chunk * 64, 64), 64), :]
@@ -183,7 +184,8 @@
 
     for c in y_cp:
         c.wait_recv()
-    zs[...] = (pm[...] + ym[0]) + (ym[1] + ym[2])
+    part = (part + ym[0].astype(F32)) + (ym[1].astype(F32) + ym[2].astype(F32))
+    zs[...] = part.astype(BF16)
     z_cp = [remote(zs, zm.at[d - 1], z_s.at[d - 1], z_r.at[d - 1], z_peer(d)) for d in range(1, NZ)]
     for c in z_cp:
         c.start()
@@ -194,7 +196,9 @@
 
     for c in z_cp:
         c.wait_recv()
-    xm[tp] = (zs[...] + zm[0]) + (zm[1] + zm[2]) + ((zm[3] + zm[4]) + (zm[5] + zm[6]))
+    for d in range(NZ - 1):
+        part = part + zm[d].astype(F32)
+    xm[tp] = part
     x_cp = [remote(xm.at[tp], xm.at[tp], x_s.at[d - 1], x_r.at[d - 1], x_peer(d)) for d in range(1, NX)]
     for c in x_cp:
         c.start()
@@ -249,22 +253,56 @@
         kvb.at[pl.ds(TOK, WINDOW), :], kvb.at[pl.ds(0, WINDOW), :], h_s.at[1], h_r.at[1], right
     )
 
-    def project(i, carry):
-        b = lax.rem(3 * i, 4)
-        base = pl.multiple_of(b * ROWS, ROWS)
-
-        def modulate(r, c2):
-            rows = pl.ds(pl.multiple_of(base + r * 64, 64), 64)
-            inv = rinv[rows, :]
-            for c in range(D // 128):
-                cols = pl.ds(c * 128, 128)
-                v = lat[rows, cols].astype(F32) * inv
-                v = v.reshape(8, 8, 128) * vec[0, :, cols][None] + vec[1, :, cols][None]
-                lin[pl.ds(pl.multiple_of(r * 64, 64), 64), cols] = v.reshape(64, 128).astype(BF16)
-            return c2
-
-        lax.fori_loop(0, ROWS // 64, modulate, 0)
-
+    side_peers = (y_peer(1), y_peer(NY - 1), z_peer(1), z_peer(NZ - 1))
+    blocks = (x_before, x_after, x_far)
+
+    def to_side(n, k):
+        rows = wo_rows(blocks[n], quarter, k // 2, 32, 32 * (k % 2))
+        return remote(rows, rows, w_s.at[4 * n + k], w_r.at[4 * n + k], side_peers[k])
+
+    def from_side(n, k):
+        rows = wo_rows(blocks[n], other, k // 2, 32, 32 * (k % 2))
+        return remote(rows, rows, w_s.at[4 * n + k], w_r.at[4 * n + k], side_peers[k])
+
+    def to_partner(n, block, q):
+        rows = wo_rows(block, q, 0, 128)
+        return remote(rows, rows, d_s.at[n], d_r.at[n], partner)
+
+    sent = []
+
+    def go(c):
+        c.start()
+        sent.append(c)
+
+    zrows = CROWS * NZ
+    near = 4 * CROWS
+
+    def pass_context(first):
+        group = (1, 7, 2) if first else (6, 3, 5, 4)
+        for d in group:
+            cz_cp[d - 1].wait_recv()
+        pieces = [cz[d - 1].astype(F32) for d in group]
+        if first:
+            pieces = [cpiece[...].astype(F32)] + pieces
+        base = 0 if first else near
+        ckv[pl.ds(base, near), :] = jnp.concatenate(pieces, axis=0).astype(BF16)
+        for d in range(1, NY):
+            k = 2 * (d - 1) + (0 if first else 1)
+            go(remote(
+                ckv.at[pl.ds(base, near), :], ckv.at[pl.ds(d * zrows + base, near), :], cy_s.at[k], cy_r.at[k],
+                y_peer(d),
+            ))
+
+    def modulate(b, lin, r):
+        rows = pl.ds(b * ROWS + r * 64, 64)
+        inv = rinv[rows, :]
+        for c in range(D // 128):
+            cols = pl.ds(c * 128, 128)
+            v = lat[rows, cols].astype(F32) * inv
+            v = v.reshape(8, 8, 128) * vec[0, :, cols][None] + vec[1, :, cols][None]
+            lin[pl.ds(r * 64, 64), cols] = v.reshape(64, 128).astype(BF16)
+
+    def project(b, lin, next_b, next_lin):
         for g in range(ROWS // GRID_W):
             at = pl.ds(g * GRID_W, GRID_W)
             row = b * (ROWS // GRID_W) + g
@@ -279,8 +317,11 @@
             inv = lax.rsqrt(jnp.mean(v * v, axis=-1, keepdims=True) + NORM_EPSILON)
             return ((v * tab[t] + swap_quarters(v) * tab[t + 1]) * inv).astype(BF16)
 
-        for n in range(3):
+        for n in (2, 0, 1):
             out = jnp.dot(lin[...], wqkv[:, pl.ds(n * 256, 256)], preferred_element_type=F32)
+            if next_b is not None:
+                for r in {2: (0,), 0: (1, 2), 1: (3,)}[n]:
+                    modulate(next_b, next_lin, r)
             first, second = out[:, :128], out[:, 128:]
             if n < 2:
                 for h, v in ((2 * n, first), (2 * n + 1, second)):
@@ -288,77 +329,36 @@
                     qb[2 * b, pl.ds(h * 128, 128), :] = t[:128]
                     qb[2 * b + 1, pl.ds(h * 128, 128), :] = t[128:]
             else:
-                rows = pl.ds(pl.multiple_of(WINDOW + base, 128), ROWS)
+                rows = pl.ds(WINDOW + b * ROWS, ROWS)
                 kvb[rows, pl.ds(0, 128)] = turned(first, 2)
                 kvb[rows, pl.ds(128, 128)] = second.astype(BF16)
 
-        @pl.when(i == 1)
-        def _():
-            halo_to_left.start()
-            halo_to_right.start()
-
-        return carry
-
-    lax.fori_loop(0, TOK // ROWS, project, 0)
-
-    def to_y(n, block):
-        return [
-            remote(
-                wo_rows(block, quarter, c, 64), wo_rows(block, quarter, c, 64),
-                w_s.at[2 * n + c], w_r.at[2 * n + c], y_peer((1, 3)[c]),
-            )
-            for c in range(2)
-        ]
-
-    def from_y(n, block):
-        return [
-            remote(
-                wo_rows(block, other, c, 64), wo_rows(block, other, c, 64),
-                w_s.at[2 * n + c], w_r.at[2 * n + c], y_peer((1, 3)[c]),
-            )
-            for c in range(2)
-        ]
-
-    def to_partner(n, block, q):
-        rows = wo_rows(block, q, 0, 128)
-        return remote(rows, rows, d_s.at[n], d_r.at[n], partner)
-
+    for r in range(ROWS // 64):
+        modulate(0, lin_a, r)
+    project(0, lin_a, 3, lin_b)
+    project(3, lin_b, 1, lin_a)
+    halo_to_left.start()
+    halo_to_right.start()
+    pass_context(True)
     for k, block in enumerate((x_before, x_after)):
         for c in range(2):
             remote(
                 own_rows(c), wo_rows(block, quarter, c, 64), s_s.at[2 * k + c], s_r.at[2 * k + c],
                 x_peer((1, 3)[k]),
             ).wait_recv()
-    r_cp = [
-        remote(
-            wo_rows(block, quarter, k, 64), wo_rows(block, quarter, k, 64), r_s.at[k], r_r.at[k],
-            x_peer((1, 3)[k]),
-        )
-        for k, block in enumerate((x_before, x_after))
-    ]
-    for c in r_cp:
-        c.start()
-    y_w = [to_y(n, block) for n, block in enumerate((x_before, x_after))]
-    d_w = [to_partner(n, block, quarter) for n, block in enumerate((x_before, x_after))]
+    for k, block in enumerate((x_before, x_after)):
+        rows = wo_rows(block, quarter, k, 64)
+        go(remote(rows, rows, r_s.at[k], r_r.at[k], x_peer((1, 3)[k])))
     for n in range(2):
-        for c in y_w[n]:
-            c.start()
-        d_w[n].start()
-
-    for c in cz_cp:
-        c.wait_recv()
-    pieces = [cpiece[...].astype(F32)] + [cz[d].astype(F32) for d in range(NZ - 1)]
-    ckv[pl.ds(0, CROWS * NZ), :] = jnp.concatenate(pieces, axis=0).astype(BF16)
-    zrows = CROWS * NZ
-    cy_cp = [
-        remote(
-            ckv.at[pl.ds(0, zrows), :], ckv.at[pl.ds(d * zrows, zrows), :], cy_s.at[d - 1], cy_r.at[d - 1],
-            y_peer(d),
-        )
-        for d in range(1, NY)
-    ]
-    for c in cy_cp:
-        c.start()
+        go(to_side(n, 2))
+        go(to_side(n, 3))
+        go(to_partner(n, blocks[n], quarter))
+    project(1, lin_a, 2, lin_b)
+    pass_context(False)
+    for n in range(2):
+        go(to_side(n, 0))
+        go(to_side(n, 1))
+    project(2, lin_b, None, None)
 
     halo_to_left.wait_recv()
     halo_to_right.wait_recv()
@@ -367,8 +367,7 @@
     k_row = lax.broadcasted_iota(jnp.int32, (stacked, WINDOW), 1)
     ahead = k_row - q_row
 
-    def window(i, carry):
-        b = lax.rem(i + 1, NBLK)
+    def window(b):
         rows = pl.ds(pl.multiple_of(b * WINDOW, WINDOW), 3 * WINDOW)
         k = kvb[rows, pl.ds(0, 128)]
         v = kvb[rows, pl.ds(128, 128)]
@@ -380,95 +379,124 @@
         e_right = jnp.where(ahead <= -no_right, e[:, 2 * WINDOW :], 0.0)
         p = jnp.concatenate([e_left, e[:, WINDOW : 2 * WINDOW], e_right], axis=1).astype(BF16)
         v2 = jnp.concatenate([v, jnp.ones((3 * WINDOW, 128), BF16)], axis=1)
-        acc[b] = jnp.dot(p, v2, preferred_element_type=F32)
+        return jnp.dot(p, v2, preferred_element_type=F32)
+
+    def window_pair(i, carry):
+        b0 = 2 * i + 1
+        b1 = lax.rem(2 * i + 2, NBLK)
+        o0, o1 = window(b0), window(b1)
+        acc[b0] = o0
+        acc[b1] = o1
         return carry
 
-    lax.fori_loop(0, NBLK, window, 0)
+    lax.fori_loop(0, NBLK // 2, window_pair, 0)
 
     for k in range(2):
         remote(
             wo_rows(x_far, quarter, k, 64), wo_rows(x_far, quarter, k, 64), r_s.at[k], r_r.at[k],
             x_peer((1, 3)[k]),
         ).wait_recv()
-    y_w.append(to_y(2, x_far))
-    d_w.append(to_partner(2, x_far, quarter))
-    for c in y_w[2]:
-        c.start()
-    d_w[2].start()
-
-    for c in cy_cp:
-        c.wait_recv()
-
-    def att_rows(i):
-        return pl.ds(pl.multiple_of(lax.rem(i, 2) * WINDOW, WINDOW), WINDOW)
-
-    my_cols = pl.ds(pl.multiple_of(tp * COLS, COLS), COLS)
-
-    def context_part(i, carry):
-        dist = lax.rem(i // 2 + 1, NX)
-        dest = lax.rem(tp + dist, NX)
-        b = 2 * dest + lax.rem(i, 2)
+    for k in range(4):
+        go(to_side(2, k))
+    go(to_partner(2, x_far, quarter))
+
+    for d in range(1, NY):
+        for f in range(2):
+            part_rows = pl.ds(d * zrows + f * near, near)
+            remote(
+                ckv.at[pl.ds(f * near, near), :], ckv.at[part_rows, :], cy_s.at[2 * (d - 1) + f],
+                cy_r.at[2 * (d - 1) + f], y_peer(d),
+            ).wait_recv()
+
+    def context_part(b):
         k = ckv[:, pl.ds(0, 128)]
         v = ckv[:, pl.ds(128, 128)]
         s = lax.dot_general(qb[b], k, (((1,), (1,)), ((), ())), preferred_element_type=F32)
         p = jnp.exp2(s).astype(BF16)
         v2 = jnp.concatenate([v, jnp.ones((CTX, 128), BF16)], axis=1)
-        o = acc[b] + jnp.dot(p, v2, preferred_element_type=F32)
-        for h in range(GROUP):
-            at = slice(h * WINDOW, (h + 1) * WINDOW)
-            sink_exp = jnp.broadcast_to(jnp.exp(sink[:, h : h + 1]), (WINDOW, 128))
-            att[i, :, pl.ds(h * 128, 128)] = (o[at, :128] / (o[at, 128:] + sink_exp)).astype(BF16)
-
-        @pl.when(i < 6)
-        def _():
-            remote(att.at[i], attx.at[att_rows(i), my_cols], a_s.at[i], a_r.at[i], {"tp": dest}).start()
-
-        @pl.when(i >= 6)
-        def _():
-            attx[att_rows(i), my_cols] = att[i]
-
+        return acc[b] + jnp.dot(p, v2, preferred_element_type=F32)
+
+    def finish(o, h):
+        at = slice(h * WINDOW, (h + 1) * WINDOW)
+        sink_exp = jnp.broadcast_to(jnp.exp(sink[:, h : h + 1]), (WINDOW, 128))
+        return (o[at, :128] / (o[at, 128:] + sink_exp)).astype(BF16)
+
+    a_cp = {}
+
+    def pair(members):
+        outs = [context_part(2 * lax.rem(tp + dist, NX) + half) for dist, half in members]
+        for (dist, half), o in zip(members, outs):
+            rows = pl.ds(half * WINDOW, WINDOW)
+            for h in range(GROUP):
+                cols = pl.ds(h * 128, 128)
+                if dist == 0:
+                    attx[0, rows, cols] = finish(o, h)
+                else:
+                    att[dist - 1, rows, cols] = finish(o, h)
+            if dist:
+                k = 2 * (dist - 1) + half
+                c = remote(att.at[dist - 1, rows, :], attx.at[dist, rows, :], a_s.at[k], a_r.at[k], x_peer(dist))
+                go(c)
+                a_cp[k] = c
+
+    pair(((1, 0), (3, 0)))
+    pair(((1, 1), (3, 1)))
+    for n in range(2):
+        for k in range(4):
+            from_side(n, k).wait_recv()
+        go(to_partner(3 + n, blocks[n], other))
+    pair(((2, 0), (2, 1)))
+    pair(((0, 0), (0, 1)))
+
+    def piece(dist, block, cols):
+        rows = pl.ds(pl.multiple_of(block * COLS, COLS), COLS)
+        return jnp.dot(attx[dist], wo[rows, cols], preferred_element_type=F32)
+
+    l_wo.wait()
+
+    def own_part(n, carry):
+        cols = pl.ds(pl.multiple_of(n * 512, 512), 512)
+        mix[:, cols] = piece(0, tp, cols)
         return carry
 
-    lax.fori_loop(0, NBLK, context_part, 0)
-
-    for n, block in enumerate((x_before, x_after, x_far)):
-        for c in from_y(n, block):
-            c.wait_recv()
-    d2_w = [to_partner(3 + n, block, other) for n, block in enumerate((x_before, x_after, x_far))]
-    for c in d2_w:
-        c.start()
-
-    a_cp = []
-    for i in range(6):
-        dist = i // 2 + 1
-        src = lax.rem(tp + NX - dist, NX)
-        cols = pl.ds(pl.multiple_of(src * COLS, COLS), COLS)
-        c = remote(
-            att.at[i], attx.at[pl.ds((i % 2) * WINDOW, WINDOW), cols], a_s.at[i], a_r.at[i],
-            {"tp": lax.rem(tp + dist, NX)},
-        )
-        c.wait_recv()
-        a_cp.append(c)
+    lax.fori_loop(0, D // 512, own_part, 0)
+
+    for k in range(4):
+        from_side(2, k).wait_recv()
+    go(to_partner(5, x_far, other))
     p_quarter, p_other = 2 * color + 1 - dp, 2 * (1 - color) + 1 - dp
-    for n, block in enumerate((x_before, x_after, x_far)):
-        to_partner(n, block, p_quarter).wait_recv()
-        to_partner(3 + n, block, p_other).wait_recv()
-    l_wo.wait()
-
-    def out_part(n, carry):
+    for n in range(2):
+        to_partner(n, blocks[n], p_quarter).wait_recv()
+        to_partner(3 + n, blocks[n], p_other).wait_recv()
+    for k in (0, 1, 4, 5):
+        a_cp[k].wait_recv()
+
+    def near_part(n, carry):
         cols = pl.ds(pl.multiple_of(n * 512, 512), 512)
-        mixed = jnp.dot(attx[...], wo[:, cols], preferred_element_type=F32)
+        mix[:, cols] = mix[:, cols] + (piece(1, x_before, cols) + piece(3, x_after, cols))
+        return carry
+
+    lax.fori_loop(0, D // 512, near_part, 0)
+
+    to_partner(2, x_far, p_quarter).wait_recv()
+    to_partner(5, x_far, p_other).wait_recv()
+    for k in (2, 3):
+        a_cp[k].wait_recv()
+
+    def far_part(n, carry):
+        cols = pl.ds(pl.multiple_of(n * 512, 512), 512)
+        mixed = mix[:, cols] + piece(2, x_far, cols)
         own = lat[pl.ds(pl.multiple_of(tp * SUB, SUB), SUB), cols].astype(F32)
         mixed = mixed.reshape(SUB // 8, 8, 512) * vec[4, :, cols][None]
         res[:, cols] = (own + mixed.reshape(SUB, 512)).astype(BF16)
         pltpu.make_async_copy(res.at[:, cols], out_h.at[:, cols], o_s.at[n]).start()
         return carry
 
-    lax.fori_loop(0, D // 512, out_part, 0)
-
-    for c in y_cp + z_cp + x_cp + cz_cp + cy_cp + r_cp + d_w + d2_w + a_cp:
+    lax.fori_loop(0, D // 512, far_part, 0)
+
+    for c in y_cp + z_cp + x_cp + cz_cp + sent:
         c.wait_send()
-    for group in s_cp + y_w:
+    for group in s_cp:
         for c in group:
             c.wait_send()
     halo_to_left.wait_send()
@@ -493,14 +521,16 @@
         vm((TOK, D), BF16), vm((CROWS, D), BF16), vm((2, D), F32), vm((1, D), F32), vm((3, 64, COLS), BF16),
         vm((D, COLS + 2 * HEAD_DIM), BF16), vm((D, D), BF16), vm((2, HEAD_DIM), F32), vm((1, GROUP), F32),
         vm((2, TOK // GRID_W, HEAD_DIM), F32), vm((2, GRID_W, HEAD_DIM), F32),
-        vm((8, COLS), F32), vm((3, 8, COLS), F32), vm((8, COLS), F32), vm((7, 8, COLS), F32),
-        vm((NX, 8, COLS), F32), vm((5, 8, D), F32), vm((TOK, 128), F32), vm((ROWS, D), BF16), vm((CROWS, D), BF16),
+        vm((8, COLS), BF16), vm((3, 8, COLS), BF16), vm((8, COLS), BF16), vm((7, 8, COLS), BF16),
+        vm((NX, 8, COLS), F32), vm((5, 8, D), F32), vm((TOK, 128), F32), vm((ROWS, D), BF16), vm((ROWS, D), BF16),
+        vm((CROWS, D), BF16),
         vm((4, ROWS, 128), F32), vm((NBLK, GROUP * WINDOW, 128), BF16), vm((TOK + 2 * WINDOW, 256), BF16),
         vm((CROWS, 256), BF16), vm((NZ - 1, CROWS, 256), BF16), vm((CTX, 256), BF16),
-        vm((NBLK, GROUP * WINDOW, 256), F32), vm((NBLK, WINDOW, COLS), BF16), vm((SUB, D), BF16), vm((SUB, D), BF16),
+        vm((NBLK, GROUP * WINDOW, 256), F32), vm((NX - 1, SUB, COLS), BF16), vm((NX, SUB, COLS), BF16),
+        vm((SUB, D), F32), vm((SUB, D), BF16),
         dma((20,)), dma((3,)), dma((3,)), dma((7,)), dma((7,)), dma((3,)), dma((3,)), dma((7,)), dma((7,)),
-        dma((3,)), dma((3,)), dma((2,)), dma((2,)), dma((6,)), dma((6,)),
-        dma((4,)), dma((4,)), dma((2,)), dma((2,)), dma((6,)), dma((6,)), dma((6,)), dma((6,)), dma((4,)),
+        dma((6,)), dma((6,)), dma((2,)), dma((2,)), dma((6,)), dma((6,)),
+        dma((4,)), dma((4,)), dma((2,)), dma((2,)), dma((12,)), dma((12,)), dma((6,)), dma((6,)), dma((4,)),
     ]
     result = pl.pallas_call(
         kernel,

time: 66.2 us -> 54.6 us (0.82)
  the two profiles are of different devices: /device:TPU:1 before, /device:TPU:6 now
where the time goes in v2:
time: 54.6 us; the launch traced here: 54.5 us
  Pallas kernels  52.2 us (96%)
  local copies, waits for them, and re-layouts  2.3 us (4%)
    pallas_call x1, Pallas kernels, per_device(): pl.pallas_call(kernel, out_shape=jax.ShapeDtypeStruct((SUB, D), BF16), in...  52.2 us
    unnamed x1, local copies, waits for them, and re-layouts  2.3 us

profile of v2, /device:TPU:6, one launch (start us, length us, event | category | flops | bytes accessed | tf_op | source)
XLA Modules:
  0.0 54.5 jit_solution(11795859510205030643)
XLA Ops:
  0.0 52.2 %shard_map.163 = bf16[256,2048]{1,0:T(8,128)(2,1)} custom-call(bf16[1024,2048]{1,0:T(8,128)(2,1)} %bitcast.8, bf16[24,2048]{1,0:T(8,128)(2,1)} %bitcast.10, f32[1,2048]{1,0:T(1,128)} %cond_h.1, f32[1,2048]{1,0:T(1,128)} %bitcast.11, f32[1,2048]{1,0:T(1,128)} %bitcast.12, bf16[64,512]{1,0:T(8,128)(2,1)} %msh_h.1, bf16[64,512]{1,0:T(8,128)(2,1)} %msc_h.1, ...), custom_call_target="tpu_custom_call" | custom-call | tf_op jit(solution)/shard_map/pallas_call | solution.py:535
  52.2 2.3 %copy.19 = bf16[1,256,2048]{2,1,0:T(8,128)(2,1)} copy(bf16[1,256,2048]{2,1,0:T(8,128)(2,1)} %bitcast.9) | data formatting | bytes 2097152

commit v3 on v2

v3 whole, which is shorter than its diff:
```python
import functools
import math

import jax
import jax.numpy as jnp
import numpy as np
from jax import lax
from jax.experimental import pallas as pl
from jax.experimental.pallas import tpu as pltpu
from jax.sharding import PartitionSpec as P

HEAD_DIM = 128
WINDOW = 128
GRID_W = 64
NORM_EPSILON = 1e-06
ROPE_BASE = 10000.0

MESH = pl.DeviceIdType.MESH
F32 = jnp.float32
BF16 = jnp.bfloat16

NY, NZ, NX = 4, 8, 4
D = 2048
COLS = 512
TOK = 1024
SUB = TOK // NX
ROWS = 256
CROWS = 24
CTX = CROWS * NY * NZ
GROUP = 4
NBLK = TOK // WINDOW
Q_FOLD = HEAD_DIM ** (-0.5) * math.log2(math.e)


def rope_tables(n_sp):
    quarter = HEAD_DIM // 4
    freq = np.float32(ROPE_BASE) ** (-np.arange(quarter, dtype=np.float32) / np.float32(quarter))
    sign = np.concatenate([-np.ones(quarter), np.ones(quarter)]).astype(np.float32)

    def table(coords):
        angles = coords.astype(np.float32)[:, None] * freq[None, :].astype(np.float32)
        angles = np.concatenate([angles, angles], axis=1).astype(np.float64)
        return np.cos(angles).astype(np.float32), np.sin(angles).astype(np.float32) * sign

    row_count = n_sp * TOK // GRID_W
    rc, rs = table(np.arange(row_count))
    cc, cs = table(np.arange(GRID_W))
    rz, cz = np.zeros_like(rc), np.zeros_like(cc)
    rows = np.stack([np.concatenate([rc, rz], 1), np.concatenate([rs, rz], 1)])
    rows = rows.reshape(2, n_sp, TOK // GRID_W, HEAD_DIM).transpose(1, 0, 2, 3)
    cols = np.stack([np.concatenate([cz, cc], 1), np.concatenate([cz, cs], 1)])
    return np.ascontiguousarray(rows), cols


def swap_quarters(v):
    lane = lax.broadcasted_iota(jnp.int32, v.shape, v.ndim - 1)
    even = (lane // 32) % 2 == 0
    return jnp.where(even, pltpu.roll(v, 96, v.ndim - 1), pltpu.roll(v, 32, v.ndim - 1))


def kernel(
    lat_h, ctx_h, cond_h, cctx_h, gain_h, msh_h, msc_h, mga_h, wq_h, wk_h, wv_h, wo_h,
    qg_h, kg_h, sink_h, rowt_h, colt_h, out_h,
    lat, ctx, cnd, gain, modw, wqkv, wo, hg, sink, rowt, colt,
    pm, zm, jm, vec, rinv, lin0, lin1, lin2, lin3, cin, tab, qb, kvb, cpiece, cz, ckv, acc, att, attx, mix, res,
    ld, m_s, m_r, c_s, c_r, h_s, h_r, a_s, a_r, w_s, w_r, o_s,
):
    sp = lax.axis_index("sp")
    tp = lax.axis_index("tp")
    dp = lax.axis_index("dp")
    y = lax.rem(sp, NY)
    z = sp // NY
    n_sp = NY * NZ

    def y_peer(d):
        return {"sp": z * NY + lax.rem(y + d, NY)}

    def z_peer(d):
        return {"sp": lax.rem(z + d, NZ) * NY + y}

    def x_peer(d):
        return {"tp": lax.rem(tp + d, NX)}

    def yx_peer(dy, dx):
        return {"sp": z * NY + lax.rem(y + dy, NY), "tp": lax.rem(tp + dx, NX)}

    partner = {"dp": 1 - dp}
    right = {"sp": lax.rem(sp + 1, n_sp)}
    left = {"sp": lax.rem(sp + n_sp - 1, n_sp)}

    def remote(src, dst, send, recv, dev):
        return pltpu.make_async_remote_copy(
            src_ref=src, dst_ref=dst, send_sem=send, recv_sem=recv, device_id=dev, device_id_type=MESH
        )

    def arrived(ref, recv):
        remote(ref, ref, m_s.at[0], recv, partner).wait_recv()

    def left_here(ref, send):
        remote(ref, ref, send, m_r.at[0], partner).wait_send()

    def load(src, dst, k):
        pltpu.make_async_copy(src, dst, ld.at[k]).start()

    def loaded(ref, k):
        pltpu.make_async_copy(ref, ref, ld.at[k]).wait()

    barrier = pltpu.get_barrier_semaphore()
    yx = [(dy, dx) for dx in range(NX) for dy in range(NY) if dy or dx]
    yx.sort(key=lambda p: -(min(p[0], NY - p[0]) + min(p[1], NX - p[1])))
    z_far = sorted(range(1, NZ), key=lambda d: -min(d, NZ - d))
    peers = [yx_peer(dy, dx) for dy, dx in yx] + [z_peer(d) for d in z_far] + [partner, left, right]
    for dev in peers:
        pl.semaphore_signal(barrier, inc=1, device_id=dev, device_id_type=MESH)

    load(msh_h, modw.at[0], 0)
    load(msc_h, modw.at[1], 0)
    load(mga_h, modw.at[2], 0)
    load(cond_h, cnd.at[pl.ds(0, 1), :], 1)
    load(cctx_h, cnd.at[pl.ds(1, 1), :], 1)
    for i in range(4):
        load(lat_h.at[pl.ds(i * 256, 256), :], lat.at[pl.ds(i * 256, 256), :], 2 + i // 2)
    load(qg_h, hg.at[pl.ds(0, 1), :], 4)
    load(kg_h, hg.at[pl.ds(1, 1), :], 4)
    load(rowt_h.at[sp], rowt, 5)
    load(colt_h, colt, 6)
    load(gain_h, gain, 7)
    load(sink_h, sink, 8)
    load(ctx_h, ctx, 9)
    load(wk_h, wqkv.at[:, pl.ds(COLS, HEAD_DIM)], 10)
    load(wv_h, wqkv.at[:, pl.ds(COLS + HEAD_DIM, HEAD_DIM)], 10)
    load(wq_h, wqkv.at[:, pl.ds(0, COLS)], 11)
    own_wo = wo.at[pl.ds(pl.multiple_of(tp * COLS, COLS), COLS), :]
    load(wo_h, own_wo, 12)

    loaded(modw, 0)
    loaded(cnd, 1)
    half = cnd[:, pl.ds(pl.multiple_of((sp // 2) * 128, 128), 128)]
    act = half / (1.0 + jnp.exp(-half))
    flipped = jnp.concatenate([act[:, 64:], act[:, :64]], axis=1)
    act = jnp.where(lax.rem(sp, 2) == 1, flipped, act)[:, :64].astype(BF16)
    part = jnp.concatenate(
        [jnp.dot(act, modw[k], preferred_element_type=F32) for k in range(3)] + [jnp.zeros((2, COLS), F32)], axis=0
    )
    pm[...] = part.astype(BF16)

    pl.semaphore_wait(barrier, len(peers))

    for d in z_far:
        remote(pm, zm.at[d - 1], m_s.at[0], m_r.at[0], z_peer(d)).start()

    color = lax.rem(y + z, 2)
    quarter = 2 * color + dp
    other = 2 * (1 - color) + dp
    x_before = lax.rem(tp + 3, NX)
    x_after = lax.rem(tp + 1, NX)
    x_far = lax.rem(tp + 2, NX)
    blocks = (x_before, x_after, x_far)

    def wo_rows(block, q, first, count):
        return wo.at[pl.ds(pl.multiple_of(block * COLS + q * 128 + first, 16), count), :]

    def send_own(first, count):
        src = wo_h.at[pl.ds(pl.multiple_of(quarter * 128 + first, 16), count), :]
        for step in (1, 3):
            remote(src, wo_rows(tp, quarter, first, count), w_s, w_r.at[0], x_peer(step)).start()

    send_own(0, 48)

    def norms(i, carry):
        rows = pl.ds(pl.multiple_of(i * 64, 64), 64)
        total = jnp.zeros((64, 128), F32)
        for c in range(D // 128):
            v = lat[rows, pl.ds(c * 128, 128)].astype(F32)
            total = total + v * v
        mean = jnp.sum(total, axis=-1, keepdims=True) * (1.0 / D)
        rinv[rows, :] = jnp.broadcast_to(lax.rsqrt(mean + NORM_EPSILON), (64, 128))
        return carry

    loaded(lat.at[pl.ds(0, 512), :], 2)
    lax.fori_loop(0, 8, norms, 0)

    loaded(hg, 4)
    loaded(rowt, 5)
    loaded(colt, 6)
    q_gain = jnp.broadcast_to(hg[0:1, :], (8, 128)) * Q_FOLD
    k_gain = jnp.broadcast_to(hg[1:2, :], (8, 128))
    q_swap, k_swap = swap_quarters(q_gain), swap_quarters(k_gain)

    def tables(row, carry):
        at = pl.ds(pl.multiple_of(row * GRID_W, GRID_W), GRID_W)
        cosine = colt[0].reshape(8, 8, 128) + rowt[0, pl.ds(row, 1), :][None]
        sine = colt[1].reshape(8, 8, 128) + rowt[1, pl.ds(row, 1), :][None]
        tab[0, at, :] = (cosine * q_gain[None]).reshape(64, 128)
        tab[1, at, :] = (sine * q_swap[None]).reshape(64, 128)
        tab[2, at, :] = (cosine * k_gain[None]).reshape(64, 128)
        tab[3, at, :] = (sine * k_swap[None]).reshape(64, 128)
        return carry

    lax.fori_loop(0, TOK // GRID_W, tables, 0)

    arrived(zm, m_r.at[0])
    for d in range(NZ - 1):
        part = part + zm[d].astype(F32)
    jm[0] = part.astype(BF16)
    for dy, dx in yx:
        remote(jm.at[0], jm.at[NY * dx + dy], m_s.at[1], m_r.at[1], yx_peer(dy, dx)).start()
    send_own(48, 80)

    loaded(lat.at[pl.ds(512, 512), :], 3)
    lax.fori_loop(8, 16, norms, 0)

    loaded(ctx, 9)
    c_total = jnp.zeros((CROWS, 128), F32)
    for c in range(D // 128):
        v = ctx[:, pl.ds(c * 128, 128)].astype(F32)
        c_total = c_total + v * v
    c_mean = jnp.sum(c_total, axis=-1, keepdims=True) * (1.0 / D)
    c_inv = jnp.broadcast_to(lax.rsqrt(c_mean + NORM_EPSILON), (CROWS, 128))
    loaded(gain, 7)
    loaded(sink, 8)
    loaded(wqkv.at[:, pl.ds(COLS, 2 * HEAD_DIM)], 10)

    arrived(jm.at[pl.ds(1, NX * NY - 1)], m_r.at[1])
    for dx in range(NX):
        m = part if dx == 0 else jm[NY * dx].astype(F32)
        for dy in range(1, NY):
            m = m + jm[NY * dx + dy].astype(F32)
        cols = pl.ds(pl.multiple_of(lax.rem(tp + NX - dx, NX) * COLS, COLS), COLS)
        g = gain[:, cols]
        for k, row in ((0, g * (1.0 + m[2:3])), (1, m[0:1]), (2, g * (1.0 + m[3:4])), (3, m[1:2]), (4, m[4:5])):
            vec[k, :, cols] = jnp.broadcast_to(row, (8, COLS))

    for c in range(D // 128):
        cols = pl.ds(c * 128, 128)
        v = ctx[:, cols].astype(F32) * c_inv
        v = v.reshape(CROWS // 8, 8, 128) * vec[2, :, cols][None] + vec[3, :, cols][None]
        cin[:, cols] = v.reshape(CROWS, 128).astype(BF16)
    kv = jnp.dot(cin[...], wqkv[:, pl.ds(COLS, 2 * HEAD_DIM)], preferred_element_type=F32)
    key = kv[:, :HEAD_DIM]
    mean = jnp.mean(key * key, axis=-1, keepdims=True)
    key = key * lax.rsqrt(mean + NORM_EPSILON) * hg[1:2, :]
    cpiece[:, pl.ds(0, HEAD_DIM)] = key.astype(BF16)
    cpiece[:, pl.ds(HEAD_DIM, HEAD_DIM)] = kv[:, HEAD_DIM:].astype(BF16)
    near_z, far_z = (1, 7, 2), (4, 5, 3, 6)
    for k, group in ((1, far_z), (0, near_z)):
        for n, d in enumerate(group):
            remote(cpiece, cz.at[3 * k + n], c_s.at[0], c_r.at[k], z_peer(d)).start()

    loaded(wqkv.at[:, pl.ds(0, COLS)], 11)
    side_peers = (y_peer(1), y_peer(NY - 1), z_peer(1), z_peer(NZ - 1))

    def to_side(n, k):
        rows = wo_rows(blocks[n], quarter, 32 * k, 32)
        remote(rows, rows, w_s, w_r.at[2 + n // 2], side_peers[k]).start()

    def to_partner(n, q):
        rows = wo_rows(blocks[n], q, 0, 128)
        remote(rows, rows, w_s, w_r.at[4 + n // 2], partner).start()

    zrows = CROWS * NZ
    near = 4 * CROWS

    def pass_context(first):
        if first:
            arrived(cz.at[pl.ds(0, 3)], c_r.at[0])
            pieces = [cpiece[...].astype(F32)] + [cz[n].astype(F32) for n in range(3)]
        else:
            arrived(cz.at[pl.ds(3, 4)], c_r.at[1])
            pieces = [cz[n].astype(F32) for n in range(3, 7)]
        base = 0 if first else near
        ckv[pl.ds(base, near), :] = jnp.concatenate(pieces, axis=0).astype(BF16)
        for d in (2, 1, 3):
            rows = pl.ds(d * zrows + base, near)
            remote(ckv.at[pl.ds(base, near), :], ckv.at[rows, :], c_s.at[1], c_r.at[2], y_peer(d)).start()

    def modulate(b, lin, r):
        rows = pl.ds(b * ROWS + r * 64, 64)
        inv = rinv[rows, :]
        for c in range(D // 128):
            cols = pl.ds(c * 128, 128)
            v = lat[rows, cols].astype(F32) * inv
            v = v.reshape(8, 8, 128) * vec[0, :, cols][None] + vec[1, :, cols][None]
            lin[pl.ds(r * 64, 64), cols] = v.reshape(64, 128).astype(BF16)

    def project(b, lin, next_b, next_lin):
        def turned(v, t):
            at = pl.ds(b * ROWS, ROWS)
            inv = lax.rsqrt(jnp.mean(v * v, axis=-1, keepdims=True) + NORM_EPSILON)
            return ((v * tab[t, at, :] + swap_quarters(v) * tab[t + 1, at, :]) * inv).astype(BF16)

        for n in (2, 0, 1):
            out = jnp.dot(lin[...], wqkv[:, pl.ds(n * 256, 256)], preferred_element_type=F32)
            if next_b is not None:
                for r in {2: (0, 1), 0: (2, 3), 1: ()}[n]:
                    modulate(next_b, next_lin, r)
            first, second = out[:, :128], out[:, 128:]
            if n < 2:
                for h, v in ((2 * n, first), (2 * n + 1, second)):
                    t = turned(v, 0)
                    qb[2 * b, pl.ds(h * 128, 128), :] = t[:128]
                    qb[2 * b + 1, pl.ds(h * 128, 128), :] = t[128:]
            else:
                rows = pl.ds(WINDOW + b * ROWS, ROWS)
                kvb[rows, pl.ds(0, 128)] = turned(first, 2)
                kvb[rows, pl.ds(128, 128)] = second.astype(BF16)

    for r in range(ROWS // 64):
        modulate(0, lin0, r)
    project(0, lin0, 3, lin1)
    project(3, lin1, 1, lin2)
    first_keys, last_keys = kvb.at[pl.ds(WINDOW, WINDOW), :], kvb.at[pl.ds(TOK, WINDOW), :]
    remote(first_keys, kvb.at[pl.ds(TOK + WINDOW, WINDOW), :], h_s, h_r.at[0], left).start()
    remote(last_keys, kvb.at[pl.ds(0, WINDOW), :], h_s, h_r.at[1], right).start()
    pass_context(True)
    arrived(wo.at[pl.ds(0, 256), :], w_r.at[0])
    for k in range(2):
        rows = wo_rows(blocks[k], quarter, 64 * k, 64)
        remote(rows, rows, w_s, w_r.at[1], x_peer((1, 3)[k])).start()
    for n in range(2):
        to_side(n, 2)
        to_side(n, 3)
        to_partner(n, quarter)
    project(1, lin2, 2, lin3)
    project(2, lin3, None, None)
    pass_context(False)
    for n in range(2):
        to_side(n, 0)
        to_side(n, 1)

    arrived(kvb.at[pl.ds(TOK + WINDOW, WINDOW), :], h_r.at[0])
    arrived(kvb.at[pl.ds(0, WINDOW), :], h_r.at[1])
    stacked = GROUP * WINDOW
    q_row = lax.rem(lax.broadcasted_iota(jnp.int32, (stacked, WINDOW), 0), WINDOW)
    k_row = lax.broadcasted_iota(jnp.int32, (stacked, WINDOW), 1)
    ahead = k_row - q_row

    def window(b):
        rows = pl.ds(pl.multiple_of(b * WINDOW, WINDOW), 3 * WINDOW)
        k = kvb[rows, pl.ds(0, 128)]
        v = kvb[rows, pl.ds(128, 128)]
        s = lax.dot_general(qb[b], k, (((1,), (1,)), ((), ())), preferred_element_type=F32)
        e = jnp.exp2(s)
        no_left = jnp.logical_and(sp == 0, b == 0).astype(jnp.int32) * (2 * WINDOW)
        no_right = jnp.logical_and(sp == n_sp - 1, b == NBLK - 1).astype(jnp.int32) * (2 * WINDOW)
        e_left = jnp.where(ahead >= no_left, e[:, :WINDOW], 0.0)
        e_right = jnp.where(ahead <= -no_right, e[:, 2 * WINDOW :], 0.0)
        p = jnp.concatenate([e_left, e[:, WINDOW : 2 * WINDOW], e_right], axis=1).astype(BF16)
        v2 = jnp.concatenate([v, jnp.ones((3 * WINDOW, 128), BF16)], axis=1)
        return jnp.dot(p, v2, preferred_element_type=F32)

    def window_pair(i, carry):
        b0 = 2 * i + 1
        b1 = lax.rem(2 * i + 2, NBLK)
        o0, o1 = window(b0), window(b1)
        acc[b0] = o0
        acc[b1] = o1
        return carry

    lax.fori_loop(0, NBLK // 2, window_pair, 0)

    arrived(ckv.at[pl.ds(zrows, 3 * zrows), :], c_r.at[2])

    def context_part(b):
        k = ckv[:, pl.ds(0, 128)]
        v = ckv[:, pl.ds(128, 128)]
        s = lax.dot_general(qb[b], k, (((1,), (1,)), ((), ())), preferred_element_type=F32)
        p = jnp.exp2(s).astype(BF16)
        v2 = jnp.concatenate([v, jnp.ones((CTX, 128), BF16)], axis=1)
        return acc[b] + jnp.dot(p, v2, preferred_element_type=F32)

    def finish(o, h):
        at = slice(h * WINDOW, (h + 1) * WINDOW)
        sink_exp = jnp.broadcast_to(jnp.exp(sink[:, h : h + 1]), (WINDOW, 128))
        return (o[at, :128] / (o[at, 128:] + sink_exp)).astype(BF16)

    def pair(members):
        outs = [context_part(2 * lax.rem(tp + dist, NX) + half) for dist, half in members]
        for (dist, half), o in zip(members, outs):
            rows = pl.ds(half * WINDOW, WINDOW)
            for h in range(GROUP):
                cols = pl.ds(h * 128, 128)
                if dist == 0:
                    attx[0, rows, cols] = finish(o, h)
                else:
                    att[dist - 1, rows, cols] = finish(o, h)
            if dist:
                k = 1 + half if dist == 2 else 0
                remote(att.at[dist - 1, rows, :], attx.at[dist, rows, :], a_s, a_r.at[k], x_peer(dist)).start()

    pair(((1, 0), (3, 0)))
    arrived(wo.at[pl.ds(0, 128), :], w_r.at[1])
    for k in range(4):
        to_side(2, k)
    to_partner(2, quarter)
    pair(((1, 1), (3, 1)))
    pair(((2, 0), (2, 1)))
    arrived(wo.at[pl.ds(0, 256), :], w_r.at[2])
    for n in range(2):
        to_partner(n, other)
    pair(((0, 0), (0, 1)))

    def piece(dist, block, cols):
        rows = pl.ds(pl.multiple_of(block * COLS, COLS), COLS)
        return jnp.dot(attx[dist], wo[rows, cols], preferred_element_type=F32)

    loaded(own_wo, 12)

    def own_part(n, carry):
        cols = pl.ds(pl.multiple_of(n * 512, 512), 512)
        mix[:, cols] = piece(0, tp, cols)
        return carry

    lax.fori_loop(0, D // 512, own_part, 0)

    arrived(wo.at[pl.ds(0, 128), :], w_r.at[3])
    to_partner(2, other)
    arrived(wo.at[pl.ds(0, 512), :], w_r.at[4])
    arrived(attx.at[pl.ds(0, 2)], a_r.at[0])

    def near_part(n, carry):
        cols = pl.ds(pl.multiple_of(n * 512, 512), 512)
        mix[:, cols] = mix[:, cols] + (piece(1, x_before, cols) + piece(3, x_after, cols))
        return carry

    lax.fori_loop(0, D // 512, near_part, 0)

    arrived(wo.at[pl.ds(0, 256), :], w_r.at[5])

    far_block = pl.ds(pl.multiple_of(x_far * COLS, COLS), COLS)
    for half in range(2):
        rows = pl.ds(half * WINDOW, WINDOW)
        arrived(attx.at[2, rows, :], a_r.at[1 + half])

        def far_part(n, carry):
            cols = pl.ds(pl.multiple_of(n * 512, 512), 512)
            mixed = mix[rows, cols] + jnp.dot(attx[2, rows, :], wo[far_block, cols], preferred_element_type=F32)
            own = lat[pl.ds(pl.multiple_of(tp * SUB + half * WINDOW, WINDOW), WINDOW), cols].astype(F32)
            mixed = mixed.reshape(WINDOW // 8, 8, 512) * vec[4, :, cols][None]
            res[rows, cols] = (own + mixed.reshape(WINDOW, 512)).astype(BF16)
            return carry

        lax.fori_loop(0, D // 512, far_part, 0)
        pltpu.make_async_copy(res.at[rows, :], out_h.at[rows, :], o_s).start()

    left_here(zm, m_s.at[0])
    left_here(jm.at[pl.ds(1, NX * NY - 1)], m_s.at[1])
    left_here(cz, c_s.at[0])
    left_here(ckv.at[pl.ds(0, 6 * near), :], c_s.at[1])
    left_here(kvb.at[pl.ds(0, 2 * WINDOW), :], h_s)
    left_here(att, a_s)
    left_here(wo.at[pl.ds(0, 1536), :], w_s)
    pltpu.make_async_copy(res, out_h, o_s).wait()


def per_device(*args):
    (latent, context, cond, ctx_cond, norm_gain, mod_shift, mod_scale, mod_gate, w_query, w_key, w_value, w_out,
     q_gain, k_gain, sinks) = args
    rows, cols = rope_tables(NY * NZ)
    operands = (
        latent[0], context[0], cond, ctx_cond.reshape(1, D), norm_gain.reshape(1, D), mod_shift, mod_scale,
        mod_gate, w_query, w_key, w_value, w_out, q_gain.reshape(1, HEAD_DIM), k_gain.reshape(1, HEAD_DIM),
        sinks.reshape(1, GROUP), jnp.asarray(rows), jnp.asarray(cols),
    )
    dma = pltpu.SemaphoreType.DMA
    vm = pltpu.VMEM
    scratch = [
        vm((TOK, D), BF16), vm((CROWS, D), BF16), vm((2, D), F32), vm((1, D), F32), vm((3, 64, COLS), BF16),
        vm((D, COLS + 2 * HEAD_DIM), BF16), vm((D, D), BF16), vm((2, HEAD_DIM), F32), vm((1, GROUP), F32),
        vm((2, TOK // GRID_W, HEAD_DIM), F32), vm((2, GRID_W, HEAD_DIM), F32),
        vm((8, COLS), BF16), vm((NZ - 1, 8, COLS), BF16), vm((NX * NY, 8, COLS), BF16), vm((5, 8, D), F32),
        vm((TOK, 128), F32), vm((ROWS, D), BF16), vm((ROWS, D), BF16), vm((ROWS, D), BF16), vm((ROWS, D), BF16),
        vm((CROWS, D), BF16), vm((4, TOK, 128), F32), vm((NBLK, GROUP * WINDOW, 128), BF16),
        vm((TOK + 2 * WINDOW, 256), BF16), vm((CROWS, 256), BF16), vm((NZ - 1, CROWS, 256), BF16), vm((CTX, 256), BF16),
        vm((NBLK, GROUP * WINDOW, 256), F32), vm((NX - 1, SUB, COLS), BF16), vm((NX, SUB, COLS), BF16),
        vm((SUB, D), F32), vm((SUB, D), BF16),
        dma((13,)), dma((2,)), dma((2,)), dma((2,)), dma((3,)), dma, dma((2,)), dma, dma((3,)), dma, dma((6,)), dma,
    ]
    result = pl.pallas_call(
        kernel,
        out_shape=jax.ShapeDtypeStruct((SUB, D), BF16),
        in_specs=[pl.BlockSpec(memory_space=pl.ANY)] * len(operands),
        out_specs=pl.BlockSpec(memory_space=pl.ANY),
        scratch_shapes=scratch,
        compiler_params=pltpu.CompilerParams(
            collective_id=0, has_side_effects=True, vmem_limit_bytes=60 * 1024 * 1024
        ),
    )(*operands)
    return result[None]


def solution(mesh):
    in_specs = (
        P("dp", "sp", None), P("dp", "sp", None), P("dp", None), P(), P(), P("sp", "tp"), P("sp", "tp"),
        P("sp", "tp"), P(None, "tp"), P(None, "tp"), P(None, "tp"), P("tp", None), P(), P(), P("tp"),
    )
    out_specs = P("dp", ("sp", "tp"), None)
    return jax.shard_map(per_device, mesh=mesh, in_specs=in_specs, out_specs=out_specs, check_vma=False)
```

time: 54.6 us -> 50.8 us (0.930)
  the two profiles are of different devices: /device:TPU:6 before, /device:TPU:64 now
where the time goes in v3:
time: 50.8 us; the launch traced here: 50.7 us
  Pallas kernels  48.4 us (95%)
  local copies, waits for them, and re-layouts  2.3 us (5%)
    pallas_call x1, Pallas kernels, per_device(): pl.pallas_call(kernel, out_shape=jax.ShapeDtypeStruct((SUB, D), BF16), in...  48.4 us
    unnamed x1, local copies, waits for them, and re-layouts  2.3 us

profile of v3, /device:TPU:64, one launch (start us, length us, event | category | flops | bytes accessed | tf_op | source)
XLA Modules:
  0.0 50.7 jit_solution(9705334712834634861)
XLA Ops:
  0.0 48.4 %shard_map.163 = bf16[256,2048]{1,0:T(8,128)(2,1)} custom-call(bf16[1024,2048]{1,0:T(8,128)(2,1)} %bitcast.8, bf16[24,2048]{1,0:T(8,128)(2,1)} %bitcast.10, f32[1,2048]{1,0:T(1,128)} %cond_h.1, f32[1,2048]{1,0:T(1,128)} %bitcast.11, f32[1,2048]{1,0:T(1,128)} %bitcast.12, bf16[64,512]{1,0:T(8,128)(2,1)} %msh_h.1, bf16[64,512]{1,0:T(8,128)(2,1)} %msc_h.1, ...), custom_call_target="tpu_custom_call" | custom-call | tf_op jit(solution)/shard_map/pallas_call | solution.py:479
  48.4 2.3 %copy.19 = bf16[1,256,2048]{2,1,0:T(8,128)(2,1)} copy(bf16[1,256,2048]{2,1,0:T(8,128)(2,1)} %bitcast.9) | data formatting | bytes 2097152
